TPU v7x, 32 devices: a whole 2x2x4 slice. The times are simulated.
32 devices in a mesh: grp: 2 (over y), sp: 8 (over z, core), tp: 2 (over x).
Axes of the slice: x: 2, y: 2, z: 4, core: 2. Of those that a mesh axis runs over, the one named last changes fastest.
Arguments:
- out_gate: bfloat16 [6144, 1024], P(('grp', 'sp'), 'tp'), parts along dimension 0, may hold values from -6 to 6
- in_gate: bfloat16 [6144, 1024], P(('grp', 'sp'), 'tp'), parts along dimension 0, may hold values from -6 to 6
- conv_input: bfloat16 [6144, 1024], P(('grp', 'sp'), 'tp'), parts along dimension 0, may hold values from -6 to 6
- doc_ids: int32 [6144], P(('grp', 'sp')), parts along dimension 0, may hold values from 0 to 3, never falling along the last dimension, each value on 1 to 1536 neighbouring positions
- residual: bfloat16 [6144, 2048], P(('grp', 'sp'), 'tp'), parts along dimension 0, may hold values from -6 to 6
- conv_taps: float32 [3, 1024], P(None, 'tp'), may hold values from -6 to 6
- mix_gain: float32 [1024], P('tp'), may hold values from 0.1 to 1.9
- out_weight: bfloat16 [1024, 2048], P('tp'), may hold values from -0.1875 to 0.1875
- ffn_gain: float32 [2048], P('tp'), may hold values from 0.1 to 1.9
- routing: int32 [6144, 2], P(('grp', 'sp')), parts along dimension 0, may hold values from 0 to 15, as said below
- route_weight: float32 [6144, 2], P(('grp', 'sp')), parts along dimension 0, may hold values from 0.2 to 1.2
- expert_gate: bfloat16 [16, 2048, 512], P('sp', None, 'tp'), may hold values from -0.125 to 0.125
- expert_up: bfloat16 [16, 2048, 512], P('sp', None, 'tp'), may hold values from -0.125 to 0.125
- expert_down: bfloat16 [16, 512, 2048], P('sp', None, 'tp'), may hold values from -0.25 to 0.25
- shared_gate: bfloat16 [2048, 512], P(None, 'tp'), may hold values from -0.125 to 0.125
- shared_up: bfloat16 [2048, 512], P(None, 'tp'), may hold values from -0.125 to 0.125
- shared_down: bfloat16 [512, 2048], P(None, 'tp'), may hold values from -0.25 to 0.25
Outputs:
- layer_out: bfloat16 [6144, 2048], P(('grp', 'sp'), 'tp'), parts along dimension 0
There are 2 independent parts, one for each index of `grp`. A program takes and returns all parts, laid end to end along the dimension named above; an argument that names none is the same for every part. Nothing has to cross between parts.
Inputs may be any that keep to these rules, and one draw needn't show every extreme that they name: `routing`: each row names 2 different experts. In each aligned block of 192 rows no expert is named by more than 48 rows, and some expert is named by exactly 48 rows. `doc_ids`: never falls along the sequence; a document holds at most 1536 positions.
All inputs are finite; a program needn't handle non-finite values.
Results may differ from a plain program's by a relative error of at most 0.017.
Values may be sent and summed in bfloat16 or wider, within the bound.
A program may use at most 64 MiB of HBM per device.

v0:
```python
import jax
import jax.numpy as jnp
from jax import lax
from jax.sharding import PartitionSpec as P

D_CONV = 1024
CONV_K = 3
TOPK = 2
EXP_DEV = 2


def from_behind(value, axis, steps):
    count = lax.axis_size(axis)
    first, last = (max(0, -steps), min(count, count - steps))
    return lax.ppermute(value, axis, [(source, source + steps) for source in range(first, last)])


def body(
    out_gate,
    in_gate,
    conv_input,
    doc_ids,
    residual,
    conv_taps,
    mix_gain,
    out_weight,
    ffn_gain,
    routing,
    route_weight,
    expert_gate,
    expert_up,
    expert_down,
    shared_gate,
    shared_up,
    shared_down,
):
    tokens = residual.shape[0]
    width = out_weight.shape[1]
    n_tp = lax.axis_size("tp")
    n_sp = lax.axis_size("sp")
    rows = tokens // n_tp
    experts = n_sp * EXP_DEV
    most = max(1, 2 * rows * TOPK // experts)
    slots = n_tp * most
    total = experts * slots
    cols = expert_down.shape[2]
    product = (in_gate.astype(jnp.float32) * conv_input.astype(jnp.float32)).astype(jnp.bfloat16)
    tail = (product[tokens - CONV_K + 1 :], doc_ids[tokens - CONV_K + 1 :].astype(jnp.bfloat16))
    prev_rows, prev_docs = from_behind((tail[0], tail[1]), "sp", 1)
    extended = jnp.concatenate([prev_rows, product], axis=0).astype(jnp.float32)
    ext_docs = jnp.concatenate([prev_docs.astype(jnp.int32), doc_ids])
    mixed = jnp.zeros(product.shape, jnp.float32)
    for k in range(CONV_K):
        keep = (ext_docs[k : k + tokens] == doc_ids)[:, None]
        mixed = mixed + jnp.where(keep, conv_taps[k] * extended[k : k + tokens], jnp.float32(0.0))
    conv_out = out_gate.astype(jnp.float32) * mixed
    squares = lax.psum(jnp.sum(conv_out * conv_out, axis=1), "tp")
    normed = (conv_out * lax.rsqrt(squares / D_CONV + 1e-06)[:, None] * mix_gain).astype(
        jnp.bfloat16
    )
    partial_value = jnp.dot(normed, out_weight, preferred_element_type=jnp.float32)
    proj = lax.psum_scatter(
        partial_value.astype(jnp.bfloat16), "tp", scatter_dimension=1, tiled=True
    ).astype(jnp.float32)
    stream = (residual.astype(jnp.float32) + proj).astype(jnp.bfloat16)
    stream32 = stream.astype(jnp.float32)
    stream_sq = lax.psum(jnp.sum(stream32 * stream32, axis=1), "tp")
    normal_cols = (stream32 * lax.rsqrt(stream_sq / width + 1e-06)[:, None] * ffn_gain).astype(
        jnp.bfloat16
    )
    flat_expert = routing.reshape(-1)
    onehot = (flat_expert[:, None] == jnp.arange(experts, dtype=jnp.int32)[None, :]).astype(
        jnp.int32
    )
    blocked = onehot.reshape(n_tp, rows * TOPK, experts)
    earlier = jnp.cumsum(blocked, axis=1) - blocked
    position = jnp.sum(earlier * blocked, axis=2).reshape(-1)
    entry = jnp.arange(tokens * TOPK, dtype=jnp.int32)
    slot = flat_expert * slots + entry // (rows * TOPK) * most + position
    table = jnp.full((total,), tokens, jnp.int32).at[slot].set(entry // TOPK)
    block_rows = lax.all_to_all(normal_cols, "tp", split_axis=0, concat_axis=1, tiled=True)
    mine = lax.dynamic_index_in_dim(
        table.reshape(n_sp, EXP_DEV, n_tp, most), lax.axis_index("tp"), 2, False
    )
    local = jnp.where(mine >= tokens, rows, mine - lax.axis_index("tp") * rows)
    padded_block = jnp.concatenate([block_rows, jnp.zeros((1, width), jnp.bfloat16)], axis=0)
    got = lax.all_to_all(padded_block[local], "sp", split_axis=0, concat_axis=0, tiled=True)
    arrived, whole = (
        lax.all_gather(got, "tp", axis=2, tiled=True),
        lax.all_gather(block_rows.reshape(1, 1, rows, width), "tp", axis=2, tiled=True),
    )
    normal = whole.reshape(tokens, width)
    gate = jnp.einsum("nesd,edh->nesh", arrived, expert_gate, preferred_element_type=jnp.float32)
    upper = jnp.einsum("nesd,edh->nesh", arrived, expert_up, preferred_element_type=jnp.float32)
    hidden = (jax.nn.silu(gate) * upper).astype(jnp.bfloat16)
    hidden_flat = hidden.reshape(n_sp * EXP_DEV * slots, hidden.shape[3])
    shared_hid = (
        jax.nn.silu(jnp.dot(normal, shared_gate, preferred_element_type=jnp.float32))
        * jnp.dot(normal, shared_up, preferred_element_type=jnp.float32)
    ).astype(jnp.bfloat16)
    expert_piece = lax.all_gather(hidden_flat, "tp", axis=1, tiled=True)
    shared_piece = lax.all_gather(shared_hid, "tp", axis=1, tiled=True)
    count = expert_piece.shape[1]
    expert_part = jnp.einsum(
        "nesh,ehd->nesd",
        expert_piece.reshape(n_sp, EXP_DEV, slots, count),
        expert_down,
        preferred_element_type=jnp.float32,
    )
    shared_part = jnp.dot(shared_piece, shared_down, preferred_element_type=jnp.float32)
    returned = lax.all_to_all(
        expert_part.astype(jnp.bfloat16), "sp", split_axis=0, concat_axis=0, tiled=True
    )
    picked = (
        returned.reshape(total, cols)[slot].astype(jnp.float32) * route_weight.reshape(-1)[:, None]
    )
    routed = jnp.sum(picked.reshape(tokens, TOPK, cols), axis=1)
    return (stream32 + shared_part + routed).astype(jnp.bfloat16)


def solution(mesh):
    return jax.shard_map(
        body,
        mesh=mesh,
        in_specs=(
            P(("grp", "sp"), "tp"),
            P(("grp", "sp"), "tp"),
            P(("grp", "sp"), "tp"),
            P(("grp", "sp")),
            P(("grp", "sp"), "tp"),
            P(None, "tp"),
            P("tp"),
            P("tp", None),
            P("tp"),
            P(("grp", "sp"), None),
            P(("grp", "sp"), None),
            P("sp", None, "tp"),
            P("sp", None, "tp"),
            P("sp", None, "tp"),
            P(None, "tp"),
            P(None, "tp"),
            P(None, "tp"),
        ),
        out_specs=P(("grp", "sp"), "tp"),
        check_vma=False,
    )
```

profile of v0, /device:TPU:0, one launch (start us, length us, event | category | flops | bytes accessed | tf_op | source)
XLA Modules:
  0.0 381.4 jit_solution(9126658122681021189)
XLA Ops:
  6.5 0.8 convert.4
  7.5 2.4 collective-permute-start
  9.9 1.2 multiply_convert_fusion.1
  11.1 4.6 %collective-permute-start.1 = (bf16[2,512]{1,0:T(2,128)(2,1)S(1)}, bf16[2,512]{1,0:T(2,128)(2,1)S(1)}, u32[]{:S(2)}, u32[]{:S(2)}) collective-permute-start(bf16[2,512]{1,0:T(2,128)(2,1)S(1)} %slice.53), channel_id=1, source_target_pairs={{0,2},{2,4},{4,6},{6,8},{8,10},{10,12},{12,14},{1,3},{3,5},{5,7},{... | collective-permute-start | bytes 6152 | tf_op jit(solution)/shard_map/ppermute | solution.py:15
  15.7 0.8 fusion.50
  16.5 0.8 pad_add_fusion
  17.3 0.8 slice_compare_fusion.1
  18.2 0.5 multiply_reduce_fusion.1
  18.7 4.9 %psum.14 = f32[384]{0:T(512)S(1)} all-reduce(f32[384]{0:T(512)S(1)} %get-tuple-element.5), channel_id=1, replica_groups=mesh['grp'=2,'sp'=8,'tp'=2] {'tp'}, use_global_device_ids=true, to_apply=%region_1.2 | all-reduce | flops 384 | bytes 3072 | tf_op jit(solution)/shard_map/psum | solution.py:57
  23.6 3.8 convolution_convert_fusion
  27.4 0.6 copy-done.8
  28.2 0.2 eq.34
  28.4 0.1 eq.38
  28.6 0.1 copy.36
  28.7 0.2 mul.157
  28.9 1.7 reduce-window.6
  31.0 3.4 scatter_custom_fusion
  34.5 19.5 %reduce-scatter.2.cloned.1.call-done = bf16[384,1024]{1,0:T(8,128)(2,1)} async-done(((bf16[384,2048]{1,0:T(8,128)(2,1)}), bf16[384,1024]{1,0:T(8,128)(2,1)}) %reduce-scatter.2.cloned.1.call-update) | async-done | bytes 786448 | tf_op jit(solution)/shard_map/reduce_scatter | solution.py:62
  54.0 1.5 fusion.5
  55.5 4.9 %psum.15 = f32[384]{0:T(512)S(1)} all-reduce(f32[384]{0:T(512)S(1)} %fusion.5), channel_id=1, replica_groups=mesh['grp'=2,'sp'=8,'tp'=2] {'tp'}, use_global_device_ids=true, to_apply=%region_4.5 | all-reduce | flops 384 | bytes 3072 | tf_op jit(solution)/shard_map/psum | solution.py:67
  60.4 2.3 fusion.7
  62.7 3.5 all-to-all-start
  66.4 9.5 %all-to-all-done = bf16[2,192,1024]{2,1,0:T(8,128)(2,1)S(1)} async-done(((bf16[2,192,1024]{2,1,0:T(8,128)(2,1)}), bf16[2,192,1024]{2,1,0:T(8,128)(2,1)S(1)}, u32[]{:S(2)}, u32[]{:S(2)}) %all-to-all-start) | async-done | bytes 786464 | tf_op jit(solution)/shard_map/all_to_all | solution.py:81
  76.0 0.8 copy-done.1
  77.0 4.3 %gather_fusion = bf16[768,2048]{1,0:T(8,128)(2,1)} fusion(bf16[193,2048]{1,0:T(8,128)(2,1)S(1)} %concatenate.11, s32[1024]{0:T(1024)S(1)} %pad_clamp_fusion.1), kind=kCustom, calls=%fused_computation | custom fusion | bytes 6294528 | tf_op jit(solution)/shard_map/gather | solution.py:87
  81.2 76.1 %all_to_all.29 = bf16[8,2,48,2048]{3,2,1,0:T(8,128)(2,1)S(1)} all-to-all(bf16[8,2,48,2048]{3,2,1,0:T(8,128)(2,1)} %bitcast.93), channel_id=1, replica_groups=mesh['grp'=2,'sp'=8,'tp'=2] {'sp'}, dimensions={0} | all-to-all | bytes 6291456 | tf_op jit(solution)/shard_map/all_to_all | solution.py:87
  157.3 2.1 copy.42
  159.5 78.4 %all-gather.6.cloned.1.call-done = bf16[8,2,96,2048]{3,2,0,1:T(8,128)(2,1)} async-done(((bf16[8,2,48,2048]{3,2,0,1:T(8,128)(2,1)}), bf16[8,2,96,2048]{3,2,0,1:T(8,128)(2,1)}) %all-gather.6.cloned.1.call-update) | async-done | bytes 6291472 | tf_op jit(solution)/shard_map/all_gather | solution.py:89
  237.9 5.3 %fusion.3 = f32[2,8,96,256]{3,2,1,0:T(8,128)S(1)} fusion(bf16[8,2,96,2048]{3,2,0,1:T(8,128)(2,1)} %all-gather.6.cloned.1.call-done, bf16[2,2048,256]{2,1,0:T(8,128)(2,1)} %param.28), kind=kOutput, calls=%fused_computation.12 | convolution fusion | flops 1610612736 | bytes 9961472 | tf_op jit(solution)/shard_map/nesd,edh->nesh/dot_general | solution.py:93
  243.3 0.5 copy-done.12
  243.7 2.0 fusion.10
  245.8 0.9 copy.43
  246.7 27.3 %all-gather.8.cloned.1.call-done = bf16[1536,512]{1,0:T(8,128)(2,1)} async-done(((bf16[1536,256]{1,0:T(8,128)(2,1)}), bf16[1536,512]{1,0:T(8,128)(2,1)}) %all-gather.8.cloned.1.call-update) | async-done | bytes 1572880 | tf_op jit(solution)/shard_map/all_gather | solution.py:101
  274.0 3.2 convert_bitcast_fusion
  277.2 2.1 copy.45
  279.3 4.7 %all-to-all-start.2 = ((bf16[8,2,96,1024]{3,2,1,0:T(8,128)(2,1)}), bf16[8,2,96,1024]{3,2,1,0:T(8,128)(2,1)}, u32[]{:S(2)}, u32[]{:S(2)}) async-start(bf16[8,2,96,1024]{3,2,1,0:T(8,128)(2,1)} %copy.45), calls=%async_computation.3 | async-start | bytes 6291456 | tf_op jit(solution)/shard_map/all_to_all | solution.py:111
  284.1 0.2 all-gather.4.cloned.1.call-start
  284.3 1.7 copy.34
  286.0 3.3 reshape.171
  289.4 27.4 %all-gather.4.cloned.1.call-done = bf16[1,1,384,2048]{3,2,1,0:T(8,128)(2,1)} async-done(((bf16[1,1,192,2048]{3,2,1,0:T(8,128)(2,1)}), bf16[1,1,384,2048]{3,2,1,0:T(8,128)(2,1)}) %all-gather.4.cloned.1.call-update) | async-done | bytes 1572880 | tf_op jit(solution)/shard_map/all_gather | solution.py:90
  316.9 2.4 fusion.16
  319.4 0.6 fusion.24
  320.0 7.1 %all_gather.13 = bf16[384,512]{1,0:T(8,128)(2,1)S(1)} all-gather(bf16[384,256]{1,0:T(8,128)(2,1)S(1)} %fusion.24), channel_id=1, replica_groups=mesh['grp'=2,'sp'=8,'tp'=2] {'tp'}, dimensions={1}, use_global_device_ids=true | all-gather | bytes 589824 | tf_op jit(solution)/shard_map/all_gather | solution.py:102
  327.1 28.6 %all-to-all-done.2 = bf16[8,2,96,1024]{3,2,1,0:T(8,128)(2,1)} async-done(((bf16[8,2,96,1024]{3,2,1,0:T(8,128)(2,1)}), bf16[8,2,96,1024]{3,2,1,0:T(8,128)(2,1)}, u32[]{:S(2)}, u32[]{:S(2)}) %all-to-all-start.2) | async-done | bytes 3145760 | tf_op jit(solution)/shard_map/all_to_all | solution.py:111
  355.7 6.9 %gather_fusion.1 = bf16[768,1024]{1,0:T(8,128)(2,1)} fusion(bf16[1536,1024]{1,0:T(8,128)(2,1)} %bitcast.21, s32[1024]{0:T(1024)S(1)} %pad_clamp_fusion), kind=kCustom, calls=%fused_computation.1 | custom fusion | bytes 3148800 | tf_op jit(solution)/shard_map/gather | solution.py:115
  362.5 4.7 %reshape.179 = f32[384,2,1024]{2,1,0:T(2,128)} reshape(bf16[768,1024]{1,0:T(8,128)(2,1)} %gather_fusion.1) | data formatting | bytes 4718592 | tf_op jit(solution)/shard_map/convert_element_type | solution.py:115
  367.3 6.0 %multiply_reduce_fusion = f32[384,1024]{1,0:T(8,128)S(1)} fusion(f32[384,2,1024]{2,1,0:T(2,128)} %reshape.179, f32[384,2]{1,0:T(8,128)S(1)} %copy.46), kind=kLoop, calls=%fused_computation.3 | loop fusion | flops 1179648 | bytes 4721664 | tf_op jit(solution)/shard_map/reduce_sum | solution.py:117
  373.4 1.5 fusion.9
  (65 shorter events, 1.4 us)
Async XLA Ops:
  6.5 267.5 %copy-start = (bf16[2,512,1024]{2,1,0:T(8,128)(2,1)S(1)}, bf16[2,512,1024]{2,1,0:T(8,128)(2,1)}, u32[]{:S(2)}) copy-start(bf16[2,512,1024]{2,1,0:T(8,128)(2,1)} %param.30) | copy-start | bytes 6291460
  6.5 11.6 %copy-start.7 = (bf16[384,512]{1,0:T(8,128)(2,1)S(1)}, bf16[384,512]{1,0:T(8,128)(2,1)}, u32[]{:S(2)}) copy-start(bf16[384,512]{1,0:T(8,128)(2,1)} %param.17) | copy-start | bytes 1179652
  6.5 47.4 %reduce-scatter.2.cloned.1.call-start = ((), (), s32[]{:S(2)}) async-start(), calls=%async_computation.4 | async-start | bytes 2359296 | tf_op jit(solution)/shard_map/reduce_scatter | solution.py:62
  7.5 9.0 %collective-permute-start = (bf16[2]{0:T(256)(128)(2,1)S(1)}, bf16[2]{0:T(256)(128)(2,1)S(1)}, u32[]{:S(2)}, u32[]{:S(2)}) collective-permute-start(bf16[2]{0:T(256)(128)(2,1)S(1)} %slice.37), channel_id=1, source_target_pairs={{0,2},{2,4},{4,6},{6,8},{8,10},{10,12},{12,14},{1,3},{3,5},{5,7},{... | collective-permute-start | bytes 20 | tf_op jit(solution)/shard_map/ppermute | solution.py:15
  11.1 6.9 %collective-permute-start.1 = (bf16[2,512]{1,0:T(2,128)(2,1)S(1)}, bf16[2,512]{1,0:T(2,128)(2,1)S(1)}, u32[]{:S(2)}, u32[]{:S(2)}) collective-permute-start(bf16[2,512]{1,0:T(2,128)(2,1)S(1)} %slice.53), channel_id=1, source_target_pairs={{0,2},{2,4},{4,6},{6,8},{8,10},{10,12},{12,14},{1,3},{3,5},{5,7},{... | collective-permute-start | bytes 6152 | tf_op jit(solution)/shard_map/ppermute | solution.py:15
  18.2 5.5 %copy-start.15 = (f32[512]{0:T(512)S(1)}, f32[512]{0:T(512)}, u32[]{:S(2)}) copy-start(f32[512]{0:T(512)} %param.23) | copy-start | bytes 6148
  27.4 0.7 copy-start.8
  27.4 26.6 %copy-start.3 = (bf16[384,1024]{1,0:T(8,128)(2,1)S(1)}, bf16[384,1024]{1,0:T(8,128)(2,1)}, u32[]{:S(2)}) copy-start(bf16[384,1024]{1,0:T(8,128)(2,1)} %param.21) | copy-start | bytes 2359300
  27.4 33.0 %copy-start.9 = (f32[1024]{0:T(1024)S(1)}, f32[1024]{0:T(1024)}, u32[]{:S(2)}) copy-start(f32[1024]{0:T(1024)} %param.25) | copy-start | bytes 12292
  62.7 13.3 %all-to-all-start = ((bf16[2,192,1024]{2,1,0:T(8,128)(2,1)}), bf16[2,192,1024]{2,1,0:T(8,128)(2,1)S(1)}, u32[]{:S(2)}, u32[]{:S(2)}) async-start(bf16[2,192,1024]{2,1,0:T(8,128)(2,1)} %bitcast.98), calls=%async_computation.1 | async-start | bytes 1572864 | tf_op jit(solution)/shard_map/all_to_all | solution.py:81
  66.2 171.7 %all-gather.6.cloned.1.call-start = ((), (), s32[]{:S(2)}) async-start(), calls=%async_computation.6 | async-start | bytes 9437184 | tf_op jit(solution)/shard_map/all_gather | solution.py:89
  76.0 0.9 copy-start.1
  159.4 114.6 %all-gather.8.cloned.1.call-start = ((), (), s32[]{:S(2)}) async-start(), calls=%async_computation.7 | async-start | bytes 2359296 | tf_op jit(solution)/shard_map/all_gather | solution.py:101
  237.9 5.4 %copy-start.11 = (bf16[8,2,96,2048]{3,2,0,1:T(8,128)(2,1)S(1)}, bf16[8,2,96,2048]{3,2,0,1:T(8,128)(2,1)}, u32[]{:S(2)}) copy-start(bf16[8,2,96,2048]{3,2,0,1:T(8,128)(2,1)} %all-gather.6.cloned.1.call-done) | copy-start | bytes 18874372
  237.9 5.8 %copy-start.12 = (bf16[2,2048,256]{2,1,0:T(8,128)(2,1)S(1)}, bf16[2,2048,256]{2,1,0:T(8,128)(2,1)}, u32[]{:S(2)}) copy-start(bf16[2,2048,256]{2,1,0:T(8,128)(2,1)} %param.29) | copy-start | bytes 6291460
  279.3 5.0 %copy-start.2 = (bf16[2,192,1024]{2,1,0:T(8,128)(2,1)S(1)}, bf16[2,192,1024]{2,1,0:T(8,128)(2,1)}, u32[]{:S(2)}) copy-start(bf16[2,192,1024]{2,1,0:T(8,128)(2,1)} %copy-done.1) | copy-start | bytes 2359300
  279.3 76.3 %all-to-all-start.2 = ((bf16[8,2,96,1024]{3,2,1,0:T(8,128)(2,1)}), bf16[8,2,96,1024]{3,2,1,0:T(8,128)(2,1)}, u32[]{:S(2)}, u32[]{:S(2)}) async-start(bf16[8,2,96,1024]{3,2,1,0:T(8,128)(2,1)} %copy.45), calls=%async_computation.3 | async-start | bytes 6291456 | tf_op jit(solution)/shard_map/all_to_all | solution.py:111
  284.1 32.8 %all-gather.4.cloned.1.call-start = ((), (), s32[]{:S(2)}) async-start(), calls=%async_computation.5 | async-start | bytes 2359296 | tf_op jit(solution)/shard_map/all_gather | solution.py:90
  286.0 3.3 copy-start.10
  316.9 2.4 copy-start.13
  316.9 2.5 copy-start.14
  367.3 6.1 %copy-start.4 = (bf16[384,1024]{1,0:T(8,128)(2,1)S(1)}, bf16[384,1024]{1,0:T(8,128)(2,1)}, u32[]{:S(2)}) copy-start(bf16[384,1024]{1,0:T(8,128)(2,1)} %param.21) | copy-start | bytes 2359300
  367.3 6.1 %copy-start.5 = (bf16[384,1024]{1,0:T(8,128)(2,1)S(1)}, bf16[384,1024]{1,0:T(8,128)(2,1)}, u32[]{:S(2)}) copy-start(bf16[384,1024]{1,0:T(8,128)(2,1)} %reduce-scatter.2.cloned.1.call-done) | copy-start | bytes 2359300
  367.3 6.1 %copy-start.6 = (bf16[512,1024]{1,0:T(8,128)(2,1)S(1)}, bf16[512,1024]{1,0:T(8,128)(2,1)}, u32[]{:S(2)}) copy-start(bf16[512,1024]{1,0:T(8,128)(2,1)} %param.33) | copy-start | bytes 3145732
Sparse Core Ops, SparseCore 0:
  27.6 26.3 reduce-scatter.1
  159.6 78.3 all-gather.5
  246.8 27.1 all-gather.7
  289.4 27.4 all-gather.3
where the time goes:
time: 382 us; the launch traced here: 381 us
  waiting for transfers between devices  191 us (50%)
  blocking collectives  93.1 us (24%)
  local copies, waits for them, and re-layouts  33.6 us (9%)
  matrix products  18.8 us (5%)
  other arithmetic  15.9 us (4%)
  starting transfers between devices  15.5 us (4%)
  between operations  13.5 us (4%)
    all_gather x1, waiting for transfers between devices, body(): lax.all_gather(got, 'tp', axis=2, tiled=True)  78.4 us
    all_to_all x1, blocking collectives, body(): lax.all_to_all(padded_block[local], 'sp', split_axis=0, concat_axis=0, ti...  76.1 us
    all_to_all x1, waiting for transfers between devices, body(): lax.all_to_all(expert_part.astype(jnp.bfloat16), 'sp', split_axis=0, conc...  28.6 us
    all_gather x1, waiting for transfers between devices, body(): lax.all_gather(block_rows.reshape(1, 1, rows, width), 'tp', axis=2, tiled...  27.4 us
    all_gather x1, waiting for transfers between devices, body(): expert_piece = lax.all_gather(hidden_flat, 'tp', axis=1, tiled=True)  27.3 us
    reduce_scatter x1, waiting for transfers between devices, body(): lax.psum_scatter(partial_value.astype(jnp.bfloat16), 'tp', scatter_dimens...  19.5 us
    all_to_all x1, waiting for transfers between devices, body(): lax.all_to_all(normal_cols, 'tp', split_axis=0, concat_axis=1, tiled=True)  9.54 us
  transfers between devices with their start and end apart: 8, of which 6 were waited for; matrix products, arithmetic and copies ran while one was open for 5% of the time, Pallas kernels for 0%

commit v1 on v0

--- a/solution.py
+++ b/solution.py
@@ -1,6 +1,10 @@
+import functools
+
 import jax
 import jax.numpy as jnp
 from jax import lax
+from jax.experimental import pallas as pl
+from jax.experimental.pallas import tpu as pltpu
 from jax.sharding import PartitionSpec as P
 
 D_CONV = 1024
@@ -118,9 +122,465 @@
     return (stream32 + shared_part + routed).astype(jnp.bfloat16)
 
 
+MESH = pl.DeviceIdType.MESH
+F32 = jnp.float32
+BF16 = jnp.bfloat16
+
+
+def silu_mul(gate, upper):
+    return (gate / (1.0 + jnp.exp(-gate)) * upper).astype(BF16)
+
+
+def mm(a, b):
+    return jnp.dot(a, b, preferred_element_type=F32)
+
+
+def moe_kernel(
+    n_z,
+    most,
+    own_ref,
+    own_meta,
+    gain_ref,
+    wg,
+    wu,
+    wd,
+    sg,
+    su,
+    sd,
+    out_ref,
+    blk,
+    meta,
+    xs,
+    hid,
+    shid,
+    ys,
+    acc,
+    outgo,
+    sib,
+    back,
+    fin,
+    send_sem,
+    recv_sem,
+    hid_send,
+    hid_recv,
+    sh_sem,
+    sib_send,
+    sib_recv,
+    back_send,
+    back_recv,
+):
+    s = lax.axis_index("sp")
+    t = lax.axis_index("tp")
+    z = s // 2
+    c = s % 2
+    rows, width = own_ref.shape
+    cols = out_ref.shape[2]
+    half = wg.shape[2]
+    lo = z > 0
+    hi = z < n_z - 1
+    up, down = {"sp": s + 2}, {"sp": s - 2}
+    other, peer = {"sp": s + 1 - 2 * c}, {"tp": 1 - t}
+    targets = (up, down, peer, other)
+
+    def slot(zq, cq, tq):
+        return (zq * 2 + cq) * 2 + tq
+
+    def zone(i):
+        return z + (1 - 2 * (i % 2)) * ((i + 1) // 2)
+
+    def valid(i):
+        zq = zone(i)
+        return (i >= 0) & (i <= 2 * n_z - 2) & (zq >= 0) & (zq < n_z)
+
+    def remote(src, dst, ssem, rsem, dev):
+        return pltpu.make_async_remote_copy(
+            src_ref=src,
+            dst_ref=dst,
+            send_sem=ssem,
+            recv_sem=rsem,
+            device_id=dev,
+            device_id_type=MESH,
+        )
+
+    def block(b, way, own=False):
+        return (
+            remote(
+                own_ref if own else blk.at[b],
+                blk.at[b],
+                send_sem.at[way, b, 0],
+                recv_sem.at[b, 0],
+                targets[way],
+            ),
+            remote(
+                own_meta if own else meta.at[b],
+                meta.at[b],
+                send_sem.at[way, b, 1],
+                recv_sem.at[b, 1],
+                targets[way],
+            ),
+        )
+
+    def start(b, way, own=False):
+        for copy in block(b, way, own):
+            copy.start()
+
+    def arrived(b):
+        for copy in block(b, 2):
+            copy.wait_recv()
+
+    def hid_copy(zq):
+        return remote(hid.at[t, zq], hid.at[t, zq], hid_send.at[zq], hid_recv.at[zq], peer)
+
+    def sh_copy():
+        return remote(shid.at[t], shid.at[t], sh_sem.at[0], sh_sem.at[1], peer)
+
+    def sib_copy(zq):
+        return remote(outgo.at[zq], sib.at[zq], sib_send.at[zq], sib_recv.at[zq], other)
+
+    def back_copy(zq, tq, to, dev):
+        return remote(
+            acc.at[zq, tq],
+            back.at[to, tq],
+            back_send.at[zq, tq],
+            back_recv.at[to, tq],
+            dev,
+        )
+
+    barrier = pltpu.get_barrier_semaphore()
+    for way, there in ((0, hi), (1, lo)):
+
+        @pl.when(there)
+        def _():
+            pl.semaphore_signal(barrier, inc=1, device_id=targets[way], device_id_type=MESH)
+
+    for way in (2, 3):
+        pl.semaphore_signal(barrier, inc=1, device_id=targets[way], device_id_type=MESH)
+    pl.semaphore_wait(barrier, 2 + lo.astype(jnp.int32) + hi.astype(jnp.int32))
+
+    mine = slot(z, c, t)
+
+    @pl.when(hi)
+    def _():
+        start(mine, 0, True)
+
+    @pl.when(lo)
+    def _():
+        start(mine, 1, True)
+
+    start(mine, 2, True)
+    start(mine, 3, True)
+    blk[mine] = own_ref[...]
+    meta[mine] = own_meta[...]
+
+    def picks(b):
+        pair = meta[b, z][:, :rows]
+        info = jnp.where(c == 0, pair[: 2 * EXP_DEV], pair[2 * EXP_DEV :])
+        place = lax.broadcasted_iota(jnp.int32, (most, rows), 0).astype(F32)
+        return info, [(info[e : e + 1] == place).astype(F32) for e in range(EXP_DEV)]
+
+    def normalise(value):
+        ms = jnp.mean(value * value, axis=1, keepdims=True)
+        return (value * lax.rsqrt(ms + 1e-06) * gain_ref[...]).astype(BF16)
+
+    def group(j):
+        return [(p, tq, c + p - 2 * c * p) for p in range(2) for tq in range(2)]
+
+    def hidden(zq):
+        for j, (p, tq, cq) in enumerate(group(zq)):
+            b = slot(zq, cq, tq)
+            _, chosen = picks(b)
+            sel = jnp.concatenate(chosen, axis=0).astype(BF16)
+            got = normalise(mm(sel, blk[b]))
+            for e in range(EXP_DEV):
+                xs[e, j * most : (j + 1) * most, :] = got[e * most : (e + 1) * most]
+        for e in range(EXP_DEV):
+            hid[t, zq, e] = silu_mul(mm(xs[e], wg[e]), mm(xs[e], wu[e]))
+
+    @pl.loop(1, 2 * n_z + 1)
+    def _(i):
+        @pl.when(valid(i))
+        def _():
+            zq = zone(i)
+            b = slot(zq, c, t)
+            arrived(b)
+
+            @pl.when(hi & (zq < z))
+            def _():
+                start(b, 0)
+
+            @pl.when(lo & (zq > z))
+            def _():
+                start(b, 1)
+
+            start(b, 2)
+            start(b, 3)
+
+        @pl.when(valid(i - 2))
+        def _():
+            zq = zone(i - 2)
+            b = slot(zq, c, 1 - t)
+            arrived(b)
+            start(b, 3)
+            arrived(slot(zq, 1 - c, t))
+            arrived(slot(zq, 1 - c, 1 - t))
+            hidden(zq)
+            hid_copy(zq).start()
+
+    for tq in range(2):
+        whole = normalise(blk[slot(z, c, tq)].astype(F32))
+        shid[t, tq] = silu_mul(mm(whole, sg[...]), mm(whole, su[...]))
+    sh_copy().start()
+
+    @pl.loop(0, 2 * n_z - 1)
+    def _(k):
+        i = 2 * n_z - 2 - k
+
+        @pl.when(valid(i))
+        def _():
+            zq = zone(i)
+            hid_copy(zq).wait_recv()
+            for e in range(EXP_DEV):
+                ys[e] = (
+                    mm(hid[0, zq, e], wd[e, :half, :]) + mm(hid[1, zq, e], wd[e, half:, :])
+                ).astype(BF16)
+            for j, (p, tq, cq) in enumerate(group(zq)):
+                info, chosen = picks(slot(zq, cq, tq))
+                parts = []
+                for e in range(EXP_DEV):
+                    weight = jnp.sum(
+                        chosen[e] * info[EXP_DEV + e : EXP_DEV + e + 1], axis=1, keepdims=True
+                    )
+                    part = ys[e, j * most : (j + 1) * most, :].astype(F32)
+                    parts.append((part * weight).astype(BF16))
+                sel = jnp.concatenate(chosen, axis=0).astype(BF16)
+                spread = lax.dot_general(
+                    sel,
+                    jnp.concatenate(parts, axis=0),
+                    (((0,), (0,)), ((), ())),
+                    preferred_element_type=F32,
+                ).astype(BF16)
+                if p == 0:
+                    acc[zq, tq] = spread
+                else:
+                    outgo[zq, tq] = spread
+            sib_copy(zq).start()
+
+    @pl.loop(0, 2 * n_z - 2)
+    def _(k):
+        i = 2 * n_z - 2 - k
+
+        @pl.when(valid(i))
+        def _():
+            zq = zone(i)
+            sib_copy(zq).wait_recv()
+            rising = zq > z
+            more = (rising & lo) | (jnp.logical_not(rising) & hi)
+            for tq in range(2):
+                both = acc[zq, tq].astype(F32) + sib[zq, tq].astype(F32)
+
+                @pl.when(more)
+                def _():
+                    back_copy(zq, tq, zq, up).wait_recv()
+                    acc[zq, tq] = (both + back[zq, tq].astype(F32)).astype(BF16)
+
+                @pl.when(jnp.logical_not(more))
+                def _():
+                    acc[zq, tq] = both.astype(BF16)
+
+                @pl.when(rising)
+                def _():
+                    back_copy(zq, tq, zq, up).start()
+
+                @pl.when(zq < z - 1)
+                def _():
+                    back_copy(zq, tq, zq, down).start()
+
+                @pl.when(zq == z - 1)
+                def _():
+                    back_copy(zq, tq, n_z, down).start()
+
+    sib_copy(z).wait_recv()
+    sh_copy().wait_recv()
+    for tq in range(2):
+        stream = blk[slot(z, c, tq), :, pl.ds(pl.multiple_of(t * cols, cols), cols)]
+        fin[tq] = (
+            stream.astype(F32)
+            + mm(shid[0, tq], sd[:half, :])
+            + mm(shid[1, tq], sd[half:, :])
+            + acc[z, tq].astype(F32)
+            + sib[z, tq].astype(F32)
+        )
+    for tq in range(2):
+
+        @pl.when(lo)
+        def _():
+            back_copy(z, tq, z, up).wait_recv()
+            fin[tq] = fin[tq] + back[z, tq].astype(F32)
+
+        @pl.when(hi)
+        def _():
+            back_copy(z, tq, n_z, up).wait_recv()
+            fin[tq] = fin[tq] + back[n_z, tq].astype(F32)
+
+        out_ref[tq] = fin[tq].astype(BF16)
+
+    @pl.loop(0, n_z)
+    def _(zq):
+        b = slot(zq, c, t)
+
+        @pl.when(hi & (zq <= z))
+        def _():
+            for copy in block(b, 0):
+                copy.wait_send()
+
+        @pl.when(lo & (zq >= z))
+        def _():
+            for copy in block(b, 1):
+                copy.wait_send()
+
+        for copy in block(b, 2) + block(b, 3) + block(slot(zq, c, 1 - t), 3):
+            copy.wait_send()
+        hid_copy(zq).wait_send()
+        sib_copy(zq).wait_send()
+
+        @pl.when(zq != z)
+        def _():
+            for tq in range(2):
+                back_copy(zq, tq, zq, up).wait_send()
+
+    sh_copy().wait_send()
+
+
+def fast(
+    out_gate,
+    in_gate,
+    conv_input,
+    doc_ids,
+    residual,
+    conv_taps,
+    mix_gain,
+    out_weight,
+    ffn_gain,
+    routing,
+    route_weight,
+    expert_gate,
+    expert_up,
+    expert_down,
+    shared_gate,
+    shared_up,
+    shared_down,
+):
+    tokens, cols = residual.shape
+    width = out_weight.shape[1]
+    n_tp, n_sp = lax.axis_size("tp"), lax.axis_size("sp")
+    n_z = n_sp // 2
+    rows = tokens // n_tp
+    experts = n_sp * EXP_DEV
+    most = max(1, 2 * rows * TOPK // experts)
+    t = lax.axis_index("tp")
+    swap = [(0, 1), (1, 0)]
+
+    def cut(value, who):
+        return lax.dynamic_slice_in_dim(value, who * rows, rows, 0)
+
+    res_other = lax.ppermute(cut(residual, 1 - t), "tp", swap)
+    product = (in_gate.astype(F32) * conv_input.astype(F32)).astype(BF16)
+    prev_rows, prev_docs = from_behind(
+        (product[tokens - CONV_K + 1 :], doc_ids[tokens - CONV_K + 1 :].astype(BF16)), "sp", 1
+    )
+    extended = jnp.concatenate([prev_rows, product], axis=0).astype(F32)
+    ext_docs = jnp.concatenate([prev_docs.astype(jnp.int32), doc_ids])
+    mixed = jnp.zeros(product.shape, F32)
+    for k in range(CONV_K):
+        keep = (ext_docs[k : k + tokens] == doc_ids)[:, None]
+        mixed = mixed + jnp.where(keep, conv_taps[k] * extended[k : k + tokens], F32(0.0))
+    conv_out = out_gate.astype(F32) * mixed
+    sums = jnp.sum(conv_out * conv_out, axis=1)
+    sums_other = lax.ppermute(sums, "tp", swap)
+    gain_other = lax.ppermute(ffn_gain, "tp", swap)
+    squares = sums + sums_other
+    first = t == 0
+    gain = jnp.concatenate(
+        [jnp.where(first, ffn_gain, gain_other), jnp.where(first, gain_other, ffn_gain)]
+    )
+    normed = (conv_out * lax.rsqrt(squares / D_CONV + 1e-06)[:, None] * mix_gain).astype(BF16)
+    given = mm(cut(normed, 1 - t), out_weight).astype(BF16)
+    taken = lax.ppermute(given, "tp", swap)
+    kept = mm(cut(normed, t), out_weight).astype(BF16)
+    res_mine = cut(residual, t)
+    res = jnp.concatenate(
+        [jnp.where(first, res_mine, res_other), jnp.where(first, res_other, res_mine)], axis=1
+    )
+    stream = (res.astype(F32) + (kept.astype(F32) + taken.astype(F32))).astype(BF16)
+
+    names = cut(routing, t)
+    weights = cut(route_weight, t)
+    hot = names[:, :, None] == jnp.arange(experts, dtype=jnp.int32)
+    named = jnp.any(hot, axis=1)
+    placed = jnp.sum(jnp.where(hot, weights[:, :, None], F32(0.0)), axis=1)
+    before = jnp.arange(rows)[:, None] > jnp.arange(rows)[None, :]
+    earlier = mm(before.astype(BF16), named.astype(BF16))
+    position = jnp.where(named, earlier, F32(-1.0))
+    info = jnp.stack([position, placed], axis=0).reshape(2, rows, n_sp, EXP_DEV)
+    info = info.transpose(2, 0, 3, 1).reshape(n_z, 4 * EXP_DEV, rows)
+    pad = -rows % 128
+    info = jnp.pad(info, ((0, 0), (0, 0), (0, pad)), constant_values=-1.0)
+
+    blocks = n_sp * n_tp
+    half = expert_gate.shape[2]
+    vm = pl.BlockSpec(memory_space=pltpu.VMEM)
+    dma = pltpu.SemaphoreType.DMA
+    out = pl.pallas_call(
+        functools.partial(moe_kernel, n_z, most),
+        out_shape=jax.ShapeDtypeStruct((n_tp, rows, cols), BF16),
+        in_specs=[vm] * 9,
+        out_specs=vm,
+        scratch_shapes=[
+            pltpu.VMEM((blocks, rows, width), BF16),
+            pltpu.VMEM((blocks,) + info.shape, F32),
+            pltpu.VMEM((EXP_DEV, 4 * most, width), BF16),
+            pltpu.VMEM((2, n_z, EXP_DEV, 4 * most, half), BF16),
+            pltpu.VMEM((2, 2, rows, half), BF16),
+            pltpu.VMEM((EXP_DEV, 4 * most, cols), BF16),
+            pltpu.VMEM((n_z, 2, rows, cols), BF16),
+            pltpu.VMEM((n_z, 2, rows, cols), BF16),
+            pltpu.VMEM((n_z, 2, rows, cols), BF16),
+            pltpu.VMEM((n_z + 1, 2, rows, cols), BF16),
+            pltpu.VMEM((2, rows, cols), F32),
+            dma((4, blocks, 2)),
+            dma((blocks, 2)),
+            dma((n_z,)),
+            dma((n_z,)),
+            dma((2,)),
+            dma((n_z,)),
+            dma((n_z,)),
+            dma((n_z, 2)),
+            dma((n_z + 1, 2)),
+        ],
+        compiler_params=pltpu.CompilerParams(
+            collective_id=0, has_side_effects=True, vmem_limit_bytes=64 * 1024 * 1024 - 65536
+        ),
+    )(
+        stream,
+        info,
+        gain[None, :],
+        expert_gate,
+        expert_up,
+        expert_down,
+        shared_gate,
+        shared_up,
+        shared_down,
+    )
+    return out.reshape(tokens, cols)
+
+
+def fits(mesh):
+    return mesh.shape["tp"] == 2 and mesh.shape["sp"] in (4, 6, 8)
+
+
 def solution(mesh):
     return jax.shard_map(
-        body,
+        fast if fits(mesh) else body,
         mesh=mesh,
         in_specs=(
             P(("grp", "sp"), "tp"),

time: 382 us -> 204 us (0.53)
  waiting for transfers between devices: 191 us -> 18.8 us
  Pallas kernels: 0 us -> 156 us
  blocking collectives: 93.1 us -> 0 us
  local copies, waits for them, and re-layouts: 33.6 us -> 6.28 us
  matrix products: 18.8 us -> 4.3 us
  between operations: 13.5 us -> 0.16 us
  other arithmetic: 15.9 us -> 6.07 us
    pallas_call x0 -> x1, Pallas kernels: none -> 156 us  [fast(): pl.pallas_call(functools.partial(moe_kernel, n_z, most), out_shape=jax.Sh...]
    all_gather x3 -> x0, waiting for transfers between devices: 133 us -> none  [the longest x1 78.4 us: body(): lax.all_gather(got, 'tp', axis=2, tiled=True)]
    all_to_all x1 -> x0, blocking collectives: 76.1 us -> none  [body(): lax.all_to_all(padded_block[local], 'sp', split_axis=0, concat_axis=0, ti...]
    all_to_all x2 -> x0, waiting for transfers between devices: 38.1 us -> none  [the longest x1 28.6 us: body(): lax.all_to_all(expert_part.astype(jnp.bfloat16), 'sp', split_axis=0, conc...]
    reduce_scatter x1 -> x0, waiting for transfers between devices: 19.5 us -> none  [body(): lax.psum_scatter(partial_value.astype(jnp.bfloat16), 'tp', scatter_dimens...]
    ppermute x0 -> x4, waiting for transfers between devices: none -> 18.8 us  [the longest x1 15 us: fast(): taken = lax.ppermute(given, 'tp', swap)]
    dot_general x7 -> x3, matrix products: 18.8 us -> 4.3 us  [mm(): return jnp.dot(a, b, preferred_element_type=F32)]
    gather x2 -> x0, local copies, waits for them, and re-layouts: 11.1 us -> none  [the longest x1 6.85 us: body(): returned.reshape(total, cols)[slot].astype(jnp.float32)]
  transfers between devices with their start and end apart: 8 -> 6, of which waited for: 6 -> 2; matrix products, arithmetic and copies ran while one was open for 5% -> 5% of each run, Pallas kernels for 0% -> 0%
where the time goes in v1:
time: 204 us
  Pallas kernels  156 us (76%)
  waiting for transfers between devices  18.8 us (9%)
  starting transfers between devices  12 us (6%)
  local copies, waits for them, and re-layouts  6.28 us (3%)
  other arithmetic  6.07 us (3%)
  matrix products  4.3 us (2%)
    pallas_call x1, Pallas kernels, fast(): pl.pallas_call(functools.partial(moe_kernel, n_z, most), out_shape=jax.Sh...  156 us
    ppermute x1, waiting for transfers between devices, fast(): taken = lax.ppermute(given, 'tp', swap)  15 us
    ppermute x2, starting transfers between devices, from_behind(): lax.ppermute(value, axis, [(source, source + steps) for source in range(f...  6.97 us
    dot_general x3, matrix products, mm(): return jnp.dot(a, b, preferred_element_type=F32)  4.3 us
  transfers between devices with their start and end apart: 6, of which 2 were waited for; matrix products, arithmetic and copies ran while one was open for 5% of the time, Pallas kernels for 0%

profile of v1, /device:TPU:0, one launch (start us, length us, event | category | flops | bytes accessed | tf_op | source)
XLA Modules:
  0.0 203.7 jit_solution(5928347074292915980)
XLA Ops:
  0.0 0.0 copy-start.2
  0.0 1.3 multiply_convert_fusion.1
  1.3 2.4 %collective-permute-start.2 = (bf16[2,512]{1,0:T(2,128)(2,1)S(1)}, bf16[2,512]{1,0:T(2,128)(2,1)S(1)}, u32[]{:S(2)}, u32[]{:S(2)}) collective-permute-start(bf16[2,512]{1,0:T(2,128)(2,1)S(1)} %slice.41), channel_id=1, source_target_pairs={{0,2},{2,4},{4,6},{6,8},{8,10},{10,12},{12,14},{1,3},{3,5},{5,7},{... | collective-permute-start | bytes 6152 | tf_op jit(solution)/shard_map/ppermute | solution.py:19
  3.7 0.7 convert.3
  4.4 0.1 slice.31
  4.4 4.6 %collective-permute-start.1 = (bf16[2]{0:T(256)(128)(2,1)S(1)}, bf16[2]{0:T(256)(128)(2,1)S(1)}, u32[]{:S(2)}, u32[]{:S(2)}) collective-permute-start(bf16[2]{0:T(256)(128)(2,1)S(1)} %slice.31), channel_id=1, source_target_pairs={{0,2},{2,4},{4,6},{6,8},{8,10},{10,12},{12,14},{1,3},{3,5},{5,7},{... | collective-permute-start | bytes 20 | tf_op jit(solution)/shard_map/ppermute | solution.py:19
  9.0 1.8 constant_dynamic-slice_fusion.2
  10.8 1.5 collective-permute-start
  12.3 0.5 collective-permute-start.5
  12.9 0.8 fusion.14
  13.7 0.8 constant_dynamic-slice_fusion.1
  14.4 0.2 convolution_select_fusion
  14.6 0.0 collective-permute-done.1
  14.6 0.8 pad_add_fusion
  15.4 0.8 slice_compare_fusion.1
  16.1 0.0 copy-start.5
  16.1 0.0 copy-start.4
  16.1 0.0 collective-permute-done.2
  16.1 0.1 maximum_convert_fusion
  16.3 0.0 copy-done.2
  16.3 0.0 copy-start
  16.3 0.5 multiply_reduce_fusion
  16.8 1.5 collective-permute-start.3
  18.3 0.0 copy-done.5
  18.3 0.1 constant_dynamic-slice_fusion
  18.4 3.8 %collective-permute-done.3 = f32[384]{0:T(512)S(1)} collective-permute-done((f32[384]{0:T(512)S(1)}, f32[384]{0:T(512)S(1)}, u32[]{:S(2)}, u32[]{:S(2)}) %collective-permute-start.3) | collective-permute-done | bytes 1568 | tf_op jit(solution)/shard_map/ppermute | solution.py:499
  22.3 0.0 copy-done.4
  22.3 0.0 copy-start.3
  22.3 0.0 copy-start.1
  22.3 0.1 multiply_convert_fusion
  22.4 0.0 copy-done
  22.4 1.5 convolution_convert_fusion
  23.9 1.5 collective-permute-start.4
  25.5 0.6 pad.4.own_meta
  26.1 0.0 collective-permute-done.5
  26.1 0.0 copy-done.3
  26.1 0.6 pad_maximum_fusion
  26.7 0.0 collective-permute-done
  26.7 0.0 copy-done.1
  26.7 1.2 broadcast_select_fusion.1
  27.9 15.0 %collective-permute-done.4 = bf16[192,2048]{1,0:T(8,128)(2,1)} collective-permute-done((bf16[192,2048]{1,0:T(8,128)(2,1)}, bf16[192,2048]{1,0:T(8,128)(2,1)}, u32[]{:S(2)}, u32[]{:S(2)}) %collective-permute-start.4) | collective-permute-done | bytes 786464 | tf_op jit(solution)/shard_map/ppermute | solution.py:508
  42.9 2.7 %add_convert_fusion.own_ref = bf16[192,2048]{1,0:T(8,128)(2,1)} fusion(bf16[192,2048]{1,0:T(8,128)(2,1)} %collective-permute-done.4, bf16[192,1024]{1,0:T(8,128)(2,1)S(1)} %get-tuple-element.8, bf16[192,1024]{1,0:T(8,128)(2,1)S(1)} %get-tuple-element.7, bf16[512,2048]{1,0:T(8,128)(2,1)S(1)} %copy-done, bf16[384,512]{1,0:T(8,128)(2,1)S(1)} %multiply_convert_fusion, ...), kind=kOutput, calls=%fused_computation.3 | convolution fusion | flops 406585344 | bytes 4653060 | tf_op jit(solution)/shard_map/dot_general | solution.py:135
  45.6 156.1 %shard_map.163 = bf16[2,192,1024]{2,1,0:T(8,128)(2,1)} custom-call(bf16[192,2048]{1,0:T(8,128)(2,1)} %add_convert_fusion.own_ref, f32[4,8,256]{2,1,0:T(8,128)} %pad.4.own_meta, f32[1,2048]{1,0:T(1,128)} %bitcast.19, bf16[2,2048,256]{2,1,0:T(8,128)(2,1)} %wg.1, bf16[2,2048,256]{2,1,0:T(8,128)(2,1)} %wu.1, bf16[2,512,1024]{2,1,0:T(8,128)(2,1)} %wd.1, ...), custom_call_target="tpu_custom_call" | custom-call | tf_op jit(solution)/shard_map/pallas_call | solution.py:533
  201.7 2.1 %copy.24 = bf16[384,1024]{1,0:T(8,128)(2,1)} copy(bf16[384,1024]{1,0:T(8,128)(2,1)} %bitcast.16) | data formatting | bytes 1572864
  (10 shorter events, 0.1 us)
Async XLA Ops:
  0.0 16.3 %copy-start.2 = (bf16[384,512]{1,0:T(8,128)(2,1)S(1)}, bf16[384,512]{1,0:T(8,128)(2,1)}, u32[]{:S(2)}) copy-start(bf16[384,512]{1,0:T(8,128)(2,1)} %param.17) | copy-start | bytes 1179652
  1.3 14.9 %collective-permute-start.2 = (bf16[2,512]{1,0:T(2,128)(2,1)S(1)}, bf16[2,512]{1,0:T(2,128)(2,1)S(1)}, u32[]{:S(2)}, u32[]{:S(2)}) collective-permute-start(bf16[2,512]{1,0:T(2,128)(2,1)S(1)} %slice.41), channel_id=1, source_target_pairs={{0,2},{2,4},{4,6},{6,8},{8,10},{10,12},{12,14},{1,3},{3,5},{5,7},{... | collective-permute-start | bytes 6152 | tf_op jit(solution)/shard_map/ppermute | solution.py:19
  4.4 10.1 %collective-permute-start.1 = (bf16[2]{0:T(256)(128)(2,1)S(1)}, bf16[2]{0:T(256)(128)(2,1)S(1)}, u32[]{:S(2)}, u32[]{:S(2)}) collective-permute-start(bf16[2]{0:T(256)(128)(2,1)S(1)} %slice.31), channel_id=1, source_target_pairs={{0,2},{2,4},{4,6},{6,8},{8,10},{10,12},{12,14},{1,3},{3,5},{5,7},{... | collective-permute-start | bytes 20 | tf_op jit(solution)/shard_map/ppermute | solution.py:19
  10.8 15.9 %collective-permute-start = (bf16[192,1024]{1,0:T(8,128)(2,1)}, bf16[192,1024]{1,0:T(8,128)(2,1)}, u32[]{:S(2)}, u32[]{:S(2)}) collective-permute-start(bf16[192,1024]{1,0:T(8,128)(2,1)} %constant_dynamic-slice_fusion.2), channel_id=1, source_target_pairs={{0,1},{1,0},{2,3},{3,2},{4,5},{5,4},{6,7},{7,6},{8,9},{9,8},{10,11... | collective-permute-start | bytes 1179656 | tf_op jit(solution)/shard_map/ppermute | solution.py:486
  12.3 13.8 %collective-permute-start.5 = (f32[1024]{0:T(1024)}, f32[1024]{0:T(1024)S(1)}, u32[]{:S(2)}, u32[]{:S(2)}) collective-permute-start(f32[1024]{0:T(1024)} %param.25), channel_id=1, source_target_pairs={{0,1},{1,0},{2,3},{3,2},{4,5},{5,4},{6,7},{7,6},{8,9},{9,8},{10,11... | collective-permute-start | bytes 12296 | tf_op jit(solution)/shard_map/ppermute | solution.py:500
  16.1 2.2 %copy-start.5 = (f32[384,2]{0,1:T(2,128)S(1)}, f32[384,2]{0,1:T(2,128)}, u32[]{:S(2)}) copy-start(f32[384,2]{0,1:T(2,128)} %param.27) | copy-start | bytes 9220
  16.1 6.1 %copy-start.4 = (f32[512]{0:T(512)S(1)}, f32[512]{0:T(512)}, u32[]{:S(2)}) copy-start(f32[512]{0:T(512)} %param.23) | copy-start | bytes 6148
  16.3 6.2 %copy-start = (bf16[512,2048]{1,0:T(8,128)(2,1)S(1)}, bf16[512,2048]{1,0:T(8,128)(2,1)}, u32[]{:S(2)}) copy-start(bf16[512,2048]{1,0:T(8,128)(2,1)} %param.24) | copy-start | bytes 6291460
  16.8 5.4 %collective-permute-start.3 = (f32[384]{0:T(512)S(1)}, f32[384]{0:T(512)S(1)}, u32[]{:S(2)}, u32[]{:S(2)}) collective-permute-start(f32[384]{0:T(512)S(1)} %get-tuple-element.5), channel_id=1, source_target_pairs={{0,1},{1,0},{2,3},{3,2},{4,5},{5,4},{6,7},{7,6},{8,9},{9,8},{10,11... | collective-permute-start | bytes 4616 | tf_op jit(solution)/shard_map/ppermute | solution.py:499
  22.3 3.9 %copy-start.3 = (f32[1024]{0:T(1024)S(1)}, f32[1024]{0:T(1024)}, u32[]{:S(2)}) copy-start(f32[1024]{0:T(1024)} %param.25) | copy-start | bytes 12292
  22.3 4.5 %copy-start.1 = (bf16[384,1024]{1,0:T(8,128)(2,1)S(1)}, bf16[384,1024]{1,0:T(8,128)(2,1)}, u32[]{:S(2)}) copy-start(bf16[384,1024]{1,0:T(8,128)(2,1)} %param.21) | copy-start | bytes 2359300
  23.9 19.0 %collective-permute-start.4 = (bf16[192,2048]{1,0:T(8,128)(2,1)}, bf16[192,2048]{1,0:T(8,128)(2,1)}, u32[]{:S(2)}, u32[]{:S(2)}) collective-permute-start(bf16[192,2048]{1,0:T(8,128)(2,1)} %convolution_convert_fusion), channel_id=1, source_target_pairs={{0,1},{1,0},{2,3},{3,2},{4,5},{5,4},{6,7},{7,6},{8,9},{9,8},{10,11... | collective-permute-start | bytes 2359304 | tf_op jit(solution)/shard_map/ppermute | solution.py:508

commit v2 on v1

--- a/solution.py
+++ b/solution.py
@@ -141,13 +141,19 @@
     own_ref,
     own_meta,
     gain_ref,
+    wg_hbm,
+    wu_hbm,
+    wd_hbm,
+    sg_hbm,
+    su_hbm,
+    sd_hbm,
+    out_ref,
     wg,
     wu,
     wd,
     sg,
     su,
     sd,
-    out_ref,
     blk,
     meta,
     xs,
@@ -168,7 +174,23 @@
     sib_recv,
     back_send,
     back_recv,
+    load_sem,
 ):
+    loads = [
+        pltpu.make_async_copy(src, dst, load_sem.at[n])
+        for n, (src, dst) in enumerate(
+            (
+                (wg_hbm, wg),
+                (wu_hbm, wu),
+                (sg_hbm, sg),
+                (su_hbm, su),
+                (wd_hbm, wd),
+                (sd_hbm, sd),
+            )
+        )
+    ]
+    for load in loads:
+        load.start()
     s = lax.axis_index("sp")
     t = lax.axis_index("tp")
     z = s // 2
@@ -176,6 +198,7 @@
     rows, width = own_ref.shape
     cols = out_ref.shape[2]
     half = wg.shape[2]
+    per, piece = acc.shape[1] // 2, acc.shape[2]
     lo = z > 0
     hi = z < n_z - 1
     up, down = {"sp": s + 2}, {"sp": s - 2}
@@ -237,14 +260,27 @@
     def sib_copy(zq):
         return remote(outgo.at[zq], sib.at[zq], sib_send.at[zq], sib_recv.at[zq], other)
 
-    def back_copy(zq, tq, to, dev):
+    def back_copy(zq, q, to, dev):
         return remote(
-            acc.at[zq, tq],
-            back.at[to, tq],
-            back_send.at[zq, tq],
-            back_recv.at[to, tq],
+            acc.at[zq, q],
+            back.at[to, q],
+            back_send.at[zq, q],
+            back_recv.at[to, q],
             dev,
         )
+
+    def pass_on(zq, q):
+        @pl.when(zq > z)
+        def _():
+            back_copy(zq, q, zq, up).start()
+
+        @pl.when(zq < z - 1)
+        def _():
+            back_copy(zq, q, zq, down).start()
+
+        @pl.when(zq == z - 1)
+        def _():
+            back_copy(zq, q, n_z, down).start()
 
     barrier = pltpu.get_barrier_semaphore()
     for way, there in ((0, hi), (1, lo)):
@@ -296,7 +332,45 @@
         for e in range(EXP_DEV):
             hid[t, zq, e] = silu_mul(mm(xs[e], wg[e]), mm(xs[e], wu[e]))
 
-    @pl.loop(1, 2 * n_z + 1)
+    def shared():
+        for tq in range(2):
+            whole = normalise(blk[slot(z, c, tq)].astype(F32))
+            shid[t, tq] = silu_mul(mm(whole, sg[...]), mm(whole, su[...]))
+
+    def results(zq):
+        hid_copy(zq).wait_recv()
+        for e in range(EXP_DEV):
+            ys[e] = (
+                mm(hid[0, zq, e], wd[e, :half, :]) + mm(hid[1, zq, e], wd[e, half:, :])
+            ).astype(BF16)
+        for j, (p, tq, cq) in enumerate(group(zq)):
+            info, chosen = picks(slot(zq, cq, tq))
+            parts = []
+            for e in range(EXP_DEV):
+                weight = jnp.sum(
+                    chosen[e] * info[EXP_DEV + e : EXP_DEV + e + 1], axis=1, keepdims=True
+                )
+                part = ys[e, j * most : (j + 1) * most, :].astype(F32)
+                parts.append((part * weight).astype(BF16))
+            sel = jnp.concatenate(chosen, axis=0).astype(BF16)
+            spread = lax.dot_general(
+                sel,
+                jnp.concatenate(parts, axis=0),
+                (((0,), (0,)), ((), ())),
+                preferred_element_type=F32,
+            ).astype(BF16)
+            into = acc if p == 0 else outgo
+            for h in range(per):
+                into[zq, tq * per + h] = spread[h * piece : (h + 1) * piece]
+        sib_copy(zq).start()
+
+    def is_end(zq):
+        return ((zq > z) & jnp.logical_not(lo)) | ((zq < z) & jnp.logical_not(hi))
+
+    for load in loads[:2]:
+        load.wait()
+
+    @pl.loop(1, 2 * n_z + 3)
     def _(i):
         @pl.when(valid(i))
         def _():
@@ -326,103 +400,79 @@
             hidden(zq)
             hid_copy(zq).start()
 
-    for tq in range(2):
-        whole = normalise(blk[slot(z, c, tq)].astype(F32))
-        shid[t, tq] = silu_mul(mm(whole, sg[...]), mm(whole, su[...]))
-    sh_copy().start()
-
-    @pl.loop(0, 2 * n_z - 1)
+        @pl.when(i == 3)
+        def _():
+            for load in loads[2:]:
+                load.wait()
+            shared()
+
+        @pl.when(i == 2 * n_z)
+        def _():
+            sh_copy().start()
+
+        @pl.when(valid(i - 4))
+        def _():
+            zq = zone(i - 4)
+            results(zq)
+
+            @pl.when(is_end(zq))
+            def _():
+                sib_copy(zq).wait_recv()
+                for q in range(2 * per):
+                    acc[zq, q] = (acc[zq, q].astype(F32) + sib[zq, q].astype(F32)).astype(BF16)
+                    pass_on(zq, q)
+
+    above = n_z - 1 - z
+    up_first = (above >= z).astype(jnp.int32)
+
+    @pl.loop(0, n_z - 1)
     def _(k):
-        i = 2 * n_z - 2 - k
-
-        @pl.when(valid(i))
-        def _():
-            zq = zone(i)
-            hid_copy(zq).wait_recv()
-            for e in range(EXP_DEV):
-                ys[e] = (
-                    mm(hid[0, zq, e], wd[e, :half, :]) + mm(hid[1, zq, e], wd[e, half:, :])
+        in_up = (k < above).astype(jnp.int32)
+        in_down = (k < z).astype(jnp.int32)
+        rise = in_up * (z + 1 + k) + (1 - in_up) * (z - 1 - (k - above))
+        fall = in_down * (z - 1 - k) + (1 - in_down) * (z + 1 + (k - z))
+        zq = up_first * rise + (1 - up_first) * fall
+
+        @pl.when(jnp.logical_not(is_end(zq)))
+        def _():
+            sib_copy(zq).wait_recv()
+            for q in range(2 * per):
+                back_copy(zq, q, zq, up).wait_recv()
+                acc[zq, q] = (
+                    acc[zq, q].astype(F32) + sib[zq, q].astype(F32) + back[zq, q].astype(F32)
                 ).astype(BF16)
-            for j, (p, tq, cq) in enumerate(group(zq)):
-                info, chosen = picks(slot(zq, cq, tq))
-                parts = []
-                for e in range(EXP_DEV):
-                    weight = jnp.sum(
-                        chosen[e] * info[EXP_DEV + e : EXP_DEV + e + 1], axis=1, keepdims=True
-                    )
-                    part = ys[e, j * most : (j + 1) * most, :].astype(F32)
-                    parts.append((part * weight).astype(BF16))
-                sel = jnp.concatenate(chosen, axis=0).astype(BF16)
-                spread = lax.dot_general(
-                    sel,
-                    jnp.concatenate(parts, axis=0),
-                    (((0,), (0,)), ((), ())),
-                    preferred_element_type=F32,
-                ).astype(BF16)
-                if p == 0:
-                    acc[zq, tq] = spread
-                else:
-                    outgo[zq, tq] = spread
-            sib_copy(zq).start()
-
-    @pl.loop(0, 2 * n_z - 2)
-    def _(k):
-        i = 2 * n_z - 2 - k
-
-        @pl.when(valid(i))
-        def _():
-            zq = zone(i)
-            sib_copy(zq).wait_recv()
-            rising = zq > z
-            more = (rising & lo) | (jnp.logical_not(rising) & hi)
-            for tq in range(2):
-                both = acc[zq, tq].astype(F32) + sib[zq, tq].astype(F32)
-
-                @pl.when(more)
-                def _():
-                    back_copy(zq, tq, zq, up).wait_recv()
-                    acc[zq, tq] = (both + back[zq, tq].astype(F32)).astype(BF16)
-
-                @pl.when(jnp.logical_not(more))
-                def _():
-                    acc[zq, tq] = both.astype(BF16)
-
-                @pl.when(rising)
-                def _():
-                    back_copy(zq, tq, zq, up).start()
-
-                @pl.when(zq < z - 1)
-                def _():
-                    back_copy(zq, tq, zq, down).start()
-
-                @pl.when(zq == z - 1)
-                def _():
-                    back_copy(zq, tq, n_z, down).start()
+                pass_on(zq, q)
 
     sib_copy(z).wait_recv()
     sh_copy().wait_recv()
     for tq in range(2):
         stream = blk[slot(z, c, tq), :, pl.ds(pl.multiple_of(t * cols, cols), cols)]
-        fin[tq] = (
+        base = (
             stream.astype(F32)
             + mm(shid[0, tq], sd[:half, :])
             + mm(shid[1, tq], sd[half:, :])
-            + acc[z, tq].astype(F32)
-            + sib[z, tq].astype(F32)
         )
-    for tq in range(2):
+        for h in range(per):
+            q = tq * per + h
+            fin[q] = (
+                base[h * piece : (h + 1) * piece]
+                + acc[z, q].astype(F32)
+                + sib[z, q].astype(F32)
+            )
+    for q in range(2 * per):
 
         @pl.when(lo)
         def _():
-            back_copy(z, tq, z, up).wait_recv()
-            fin[tq] = fin[tq] + back[z, tq].astype(F32)
+            back_copy(z, q, z, up).wait_recv()
+            fin[q] = fin[q] + back[z, q].astype(F32)
 
         @pl.when(hi)
         def _():
-            back_copy(z, tq, n_z, up).wait_recv()
-            fin[tq] = fin[tq] + back[n_z, tq].astype(F32)
-
-        out_ref[tq] = fin[tq].astype(BF16)
+            back_copy(z, q, n_z, up).wait_recv()
+            fin[q] = fin[q] + back[n_z, q].astype(F32)
+
+        tq, h = divmod(q, per)
+        out_ref[tq, h * piece : (h + 1) * piece, :] = fin[q].astype(BF16)
 
     @pl.loop(0, n_z)
     def _(zq):
@@ -445,8 +495,8 @@
 
         @pl.when(zq != z)
         def _():
-            for tq in range(2):
-                back_copy(zq, tq, zq, up).wait_send()
+            for q in range(2 * per):
+                back_copy(zq, q, zq, up).wait_send()
 
     sh_copy().wait_send()
 
@@ -506,7 +556,7 @@
     normed = (conv_out * lax.rsqrt(squares / D_CONV + 1e-06)[:, None] * mix_gain).astype(BF16)
     given = mm(cut(normed, 1 - t), out_weight).astype(BF16)
     taken = lax.ppermute(given, "tp", swap)
-    kept = mm(cut(normed, t), out_weight).astype(BF16)
+    kept = lax.optimization_barrier(mm(cut(normed, t), out_weight).astype(BF16))
     res_mine = cut(residual, t)
     res = jnp.concatenate(
         [jnp.where(first, res_mine, res_other), jnp.where(first, res_other, res_mine)], axis=1
@@ -526,6 +576,8 @@
     pad = -rows % 128
     info = jnp.pad(info, ((0, 0), (0, 0), (0, pad)), constant_values=-1.0)
 
+    per = 2
+    piece = rows // per
     blocks = n_sp * n_tp
     half = expert_gate.shape[2]
     vm = pl.BlockSpec(memory_space=pltpu.VMEM)
@@ -533,20 +585,26 @@
     out = pl.pallas_call(
         functools.partial(moe_kernel, n_z, most),
         out_shape=jax.ShapeDtypeStruct((n_tp, rows, cols), BF16),
-        in_specs=[vm] * 9,
+        in_specs=[vm] * 3 + [pl.BlockSpec(memory_space=pl.ANY)] * 6,
         out_specs=vm,
         scratch_shapes=[
+            pltpu.VMEM(expert_gate.shape, BF16),
+            pltpu.VMEM(expert_up.shape, BF16),
+            pltpu.VMEM(expert_down.shape, BF16),
+            pltpu.VMEM(shared_gate.shape, BF16),
+            pltpu.VMEM(shared_up.shape, BF16),
+            pltpu.VMEM(shared_down.shape, BF16),
             pltpu.VMEM((blocks, rows, width), BF16),
             pltpu.VMEM((blocks,) + info.shape, F32),
             pltpu.VMEM((EXP_DEV, 4 * most, width), BF16),
             pltpu.VMEM((2, n_z, EXP_DEV, 4 * most, half), BF16),
             pltpu.VMEM((2, 2, rows, half), BF16),
             pltpu.VMEM((EXP_DEV, 4 * most, cols), BF16),
-            pltpu.VMEM((n_z, 2, rows, cols), BF16),
-            pltpu.VMEM((n_z, 2, rows, cols), BF16),
-            pltpu.VMEM((n_z, 2, rows, cols), BF16),
-            pltpu.VMEM((n_z + 1, 2, rows, cols), BF16),
-            pltpu.VMEM((2, rows, cols), F32),
+            pltpu.VMEM((n_z, 2 * per, piece, cols), BF16),
+            pltpu.VMEM((n_z, 2 * per, piece, cols), BF16),
+            pltpu.VMEM((n_z, 2 * per, piece, cols), BF16),
+            pltpu.VMEM((n_z + 1, 2 * per, piece, cols), BF16),
+            pltpu.VMEM((2 * per, piece, cols), F32),
             dma((4, blocks, 2)),
             dma((blocks, 2)),
             dma((n_z,)),
@@ -554,8 +612,9 @@
             dma((2,)),
             dma((n_z,)),
             dma((n_z,)),
-            dma((n_z, 2)),
-            dma((n_z + 1, 2)),
+            dma((n_z, 2 * per)),
+            dma((n_z + 1, 2 * per)),
+            dma((6,)),
         ],
         compiler_params=pltpu.CompilerParams(
             collective_id=0, has_side_effects=True, vmem_limit_bytes=64 * 1024 * 1024 - 65536

time: 204 us -> 194 us (0.951)
  Pallas kernels: 156 us -> 148 us
  matrix products: 4.3 us -> 1.31 us
    pallas_call x1, Pallas kernels: 156 us -> 148 us  [fast(): pl.pallas_call(functools.partial(moe_kernel, n_z, most), out_shape=jax.Sh...]
    dot_general x3, matrix products: 4.3 us -> 1.31 us  [mm(): return jnp.dot(a, b, preferred_element_type=F32)]
where the time goes in v2:
time: 194 us; the launch traced here: 193 us
  Pallas kernels  148 us (76%)
  waiting for transfers between devices  18.3 us (9%)
  starting transfers between devices  12.1 us (6%)
  local copies, waits for them, and re-layouts  6.96 us (4%)
  other arithmetic  6.1 us (3%)
    pallas_call x1, Pallas kernels, fast(): pl.pallas_call(functools.partial(moe_kernel, n_z, most), out_shape=jax.Sh...  148 us
    ppermute x1, waiting for transfers between devices, fast(): taken = lax.ppermute(given, 'tp', swap)  15.7 us
    ppermute x2, starting transfers between devices, from_behind(): lax.ppermute(value, axis, [(source, source + steps) for source in range(f...  6.97 us
  transfers between devices with their start and end apart: 6, of which 2 were waited for; matrix products, arithmetic and copies ran while one was open for 5% of the time, Pallas kernels for 0%

profile of v2, /device:TPU:0, one launch (start us, length us, event | category | flops | bytes accessed | tf_op | source)
XLA Modules:
  0.0 193.2 jit_solution(8850769896329394971)
XLA Ops:
  0.0 0.0 copy-start.2
  0.0 1.2 multiply_convert_fusion.1
  1.2 2.4 %collective-permute-start.2 = (bf16[2,512]{1,0:T(2,128)(2,1)S(1)}, bf16[2,512]{1,0:T(2,128)(2,1)S(1)}, u32[]{:S(2)}, u32[]{:S(2)}) collective-permute-start(bf16[2,512]{1,0:T(2,128)(2,1)S(1)} %slice.41), channel_id=1, source_target_pairs={{0,2},{2,4},{4,6},{6,8},{8,10},{10,12},{12,14},{1,3},{3,5},{5,7},{... | collective-permute-start | bytes 6152 | tf_op jit(solution)/shard_map/ppermute | solution.py:19
  3.6 0.7 convert.3
  4.3 0.1 slice.31
  4.4 4.6 %collective-permute-start.1 = (bf16[2]{0:T(256)(128)(2,1)S(1)}, bf16[2]{0:T(256)(128)(2,1)S(1)}, u32[]{:S(2)}, u32[]{:S(2)}) collective-permute-start(bf16[2]{0:T(256)(128)(2,1)S(1)} %slice.31), channel_id=1, source_target_pairs={{0,2},{2,4},{4,6},{6,8},{8,10},{10,12},{12,14},{1,3},{3,5},{5,7},{... | collective-permute-start | bytes 20 | tf_op jit(solution)/shard_map/ppermute | solution.py:19
  9.0 1.8 constant_dynamic-slice_fusion.2
  10.8 1.5 collective-permute-start
  12.3 0.5 collective-permute-start.5
  12.8 0.8 fusion.11
  13.6 0.8 constant_dynamic-slice_fusion.1
  14.4 0.8 constant_dynamic-slice_fusion
  15.2 0.1 convolution_select_fusion
  15.4 0.0 collective-permute-done.1
  15.4 0.0 copy-done.2
  15.4 0.1 pad_add_fusion
  15.5 0.1 slice_compare_fusion.1
  15.6 0.0 collective-permute-done.2
  15.6 0.1 maximum_convert_fusion
  15.7 0.0 copy-start.4
  15.7 0.0 copy-start
  15.7 1.7 multiply_reduce_fusion
  17.4 1.5 collective-permute-start.3
  19.0 0.6 pad.4.own_meta
  19.6 2.6 %collective-permute-done.3 = f32[384]{0:T(512)S(1)} collective-permute-done((f32[384]{0:T(512)S(1)}, f32[384]{0:T(512)S(1)}, u32[]{:S(2)}, u32[]{:S(2)}) %collective-permute-start.3) | collective-permute-done | bytes 1568 | tf_op jit(solution)/shard_map/ppermute | solution.py:549
  22.2 0.0 copy-done.4
  22.2 0.1 multiply_convert_fusion
  22.3 0.0 copy-done
  22.3 0.6 convolution_convert_fusion
  22.9 0.0 copy-start.3
  22.9 0.0 copy-start.1
  22.9 1.6 collective-permute-start.4
  24.5 0.6 convolution_convert_fusion.1
  25.1 0.0 collective-permute-done.5
  25.1 0.0 copy-done.3
  25.1 0.6 pad_maximum_fusion
  25.7 0.0 collective-permute-done
  25.7 0.0 copy-done.1
  25.7 0.2 broadcast_select_fusion.1
  25.9 15.7 %collective-permute-done.4 = bf16[192,2048]{1,0:T(8,128)(2,1)S(1)} collective-permute-done((bf16[192,2048]{1,0:T(8,128)(2,1)S(1)}, bf16[192,2048]{1,0:T(8,128)(2,1)S(1)}, u32[]{:S(2)}, u32[]{:S(2)}) %collective-permute-start.4) | collective-permute-done | bytes 786464 | tf_op jit(solution)/shard_map/ppermute | solution.py:558
  41.6 1.3 add_convert_fusion.own_ref
  42.9 148.3 %shard_map.163 = bf16[2,192,1024]{2,1,0:T(8,128)(2,1)} custom-call(bf16[192,2048]{1,0:T(8,128)(2,1)} %add_convert_fusion.own_ref, f32[4,8,256]{2,1,0:T(8,128)} %pad.4.own_meta, f32[1,2048]{1,0:T(1,128)} %bitcast.19, bf16[2,2048,256]{2,1,0:T(8,128)(2,1)} %wg_hbm.1, bf16[2,2048,256]{2,1,0:T(8,128)(2,1)} %wu_hbm.1, bf16[2,512,1024]{2,1,0:T(8,128)(2,1)} %wd_hbm.1, ...), custom_call_target="tpu_custom_call" | custom-call | tf_op jit(solution)/shard_map/pallas_call | solution.py:585
  191.2 2.1 %copy.24 = bf16[384,1024]{1,0:T(8,128)(2,1)} copy(bf16[384,1024]{1,0:T(8,128)(2,1)} %bitcast.16) | data formatting | bytes 1572864
  (10 shorter events, 0.1 us)
Async XLA Ops:
  0.0 15.4 %copy-start.2 = (s32[384]{0:T(512)S(1)}, s32[384]{0:T(512)}, u32[]{:S(2)}) copy-start(s32[384]{0:T(512)} %param.20) | copy-start | bytes 4612
  1.2 14.3 %collective-permute-start.2 = (bf16[2,512]{1,0:T(2,128)(2,1)S(1)}, bf16[2,512]{1,0:T(2,128)(2,1)S(1)}, u32[]{:S(2)}, u32[]{:S(2)}) collective-permute-start(bf16[2,512]{1,0:T(2,128)(2,1)S(1)} %slice.41), channel_id=1, source_target_pairs={{0,2},{2,4},{4,6},{6,8},{8,10},{10,12},{12,14},{1,3},{3,5},{5,7},{... | collective-permute-start | bytes 6152 | tf_op jit(solution)/shard_map/ppermute | solution.py:19
  4.4 11.0 %collective-permute-start.1 = (bf16[2]{0:T(256)(128)(2,1)S(1)}, bf16[2]{0:T(256)(128)(2,1)S(1)}, u32[]{:S(2)}, u32[]{:S(2)}) collective-permute-start(bf16[2]{0:T(256)(128)(2,1)S(1)} %slice.31), channel_id=1, source_target_pairs={{0,2},{2,4},{4,6},{6,8},{8,10},{10,12},{12,14},{1,3},{3,5},{5,7},{... | collective-permute-start | bytes 20 | tf_op jit(solution)/shard_map/ppermute | solution.py:19
  10.8 14.9 %collective-permute-start = (bf16[192,1024]{1,0:T(8,128)(2,1)}, bf16[192,1024]{1,0:T(8,128)(2,1)S(1)}, u32[]{:S(2)}, u32[]{:S(2)}) collective-permute-start(bf16[192,1024]{1,0:T(8,128)(2,1)} %constant_dynamic-slice_fusion.2), channel_id=1, source_target_pairs={{0,1},{1,0},{2,3},{3,2},{4,5},{5,4},{6,7},{7,6},{8,9},{9,8},{10,11... | collective-permute-start | bytes 1179656 | tf_op jit(solution)/shard_map/ppermute | solution.py:536
  12.3 12.8 %collective-permute-start.5 = (f32[1024]{0:T(1024)}, f32[1024]{0:T(1024)S(1)}, u32[]{:S(2)}, u32[]{:S(2)}) collective-permute-start(f32[1024]{0:T(1024)} %param.25), channel_id=1, source_target_pairs={{0,1},{1,0},{2,3},{3,2},{4,5},{5,4},{6,7},{7,6},{8,9},{9,8},{10,11... | collective-permute-start | bytes 12296 | tf_op jit(solution)/shard_map/ppermute | solution.py:550
  15.7 6.5 %copy-start.4 = (f32[512]{0:T(512)S(1)}, f32[512]{0:T(512)}, u32[]{:S(2)}) copy-start(f32[512]{0:T(512)} %param.23) | copy-start | bytes 6148
  15.7 6.6 %copy-start = (bf16[512,2048]{1,0:T(8,128)(2,1)S(1)}, bf16[512,2048]{1,0:T(8,128)(2,1)}, u32[]{:S(2)}) copy-start(bf16[512,2048]{1,0:T(8,128)(2,1)} %param.24) | copy-start | bytes 6291460
  17.4 4.8 %collective-permute-start.3 = (f32[384]{0:T(512)S(1)}, f32[384]{0:T(512)S(1)}, u32[]{:S(2)}, u32[]{:S(2)}) collective-permute-start(f32[384]{0:T(512)S(1)} %get-tuple-element.5), channel_id=1, source_target_pairs={{0,1},{1,0},{2,3},{3,2},{4,5},{5,4},{6,7},{7,6},{8,9},{9,8},{10,11... | collective-permute-start | bytes 4616 | tf_op jit(solution)/shard_map/ppermute | solution.py:549
  22.9 2.2 %copy-start.3 = (f32[1024]{0:T(1024)S(1)}, f32[1024]{0:T(1024)}, u32[]{:S(2)}) copy-start(f32[1024]{0:T(1024)} %param.25) | copy-start | bytes 12292
  22.9 2.8 %copy-start.1 = (bf16[384,1024]{1,0:T(8,128)(2,1)S(1)}, bf16[384,1024]{1,0:T(8,128)(2,1)}, u32[]{:S(2)}) copy-start(bf16[384,1024]{1,0:T(8,128)(2,1)} %param.21) | copy-start | bytes 2359300
  22.9 18.7 %collective-permute-start.4 = (bf16[192,2048]{1,0:T(8,128)(2,1)S(1)}, bf16[192,2048]{1,0:T(8,128)(2,1)S(1)}, u32[]{:S(2)}, u32[]{:S(2)}) collective-permute-start(bf16[192,2048]{1,0:T(8,128)(2,1)S(1)} %convolution_convert_fusion), channel_id=1, source_target_pairs={{0,1},{1,0},{2,3},{3,2},{4,5},{5,4},{6,7},{7,6},{8,9},{9,8},{10,11... | collective-permute-start | bytes 2359304 | tf_op jit(solution)/shard_map/ppermute | solution.py:558

commit v3 on v2

--- a/solution.py
+++ b/solution.py
@@ -425,23 +425,31 @@
     above = n_z - 1 - z
     up_first = (above >= z).astype(jnp.int32)
 
-    @pl.loop(0, n_z - 1)
-    def _(k):
+    def through(k):
         in_up = (k < above).astype(jnp.int32)
         in_down = (k < z).astype(jnp.int32)
         rise = in_up * (z + 1 + k) + (1 - in_up) * (z - 1 - (k - above))
         fall = in_down * (z - 1 - k) + (1 - in_down) * (z + 1 + (k - z))
-        zq = up_first * rise + (1 - up_first) * fall
+        return up_first * rise + (1 - up_first) * fall
+
+    def relay(k, q):
+        zq = through(k)
 
         @pl.when(jnp.logical_not(is_end(zq)))
         def _():
-            sib_copy(zq).wait_recv()
-            for q in range(2 * per):
-                back_copy(zq, q, zq, up).wait_recv()
-                acc[zq, q] = (
-                    acc[zq, q].astype(F32) + sib[zq, q].astype(F32) + back[zq, q].astype(F32)
-                ).astype(BF16)
-                pass_on(zq, q)
+            if q == 0:
+                sib_copy(zq).wait_recv()
+            back_copy(zq, q, zq, up).wait_recv()
+            acc[zq, q] = (
+                acc[zq, q].astype(F32) + sib[zq, q].astype(F32) + back[zq, q].astype(F32)
+            ).astype(BF16)
+            pass_on(zq, q)
+
+    for q in range(2 * per):
+        relay(0, q)
+    for q in range(2 * per):
+        for k in range(1, n_z - 1):
+            relay(k, q)
 
     sib_copy(z).wait_recv()
     sh_copy().wait_recv()
@@ -576,7 +584,7 @@
     pad = -rows % 128
     info = jnp.pad(info, ((0, 0), (0, 0), (0, pad)), constant_values=-1.0)
 
-    per = 2
+    per = 4 if rows % 64 == 0 else 1
     piece = rows // per
     blocks = n_sp * n_tp
     half = expert_gate.shape[2]

time: 194 us -> 198 us (1.021)
  Pallas kernels: 148 us -> 152 us
    pallas_call x1, Pallas kernels: 148 us -> 152 us  [fast(): pl.pallas_call(functools.partial(moe_kernel, n_z, most), out_shape=jax.Sh...]
where the time goes in v3:
time: 198 us; the launch traced here: 197 us
  Pallas kernels  152 us (77%)
  waiting for transfers between devices  18.3 us (9%)
  starting transfers between devices  12.1 us (6%)
  local copies, waits for them, and re-layouts  6.96 us (4%)
  other arithmetic  6.1 us (3%)
    pallas_call x1, Pallas kernels, fast(): pl.pallas_call(functools.partial(moe_kernel, n_z, most), out_shape=jax.Sh...  152 us
    ppermute x1, waiting for transfers between devices, fast(): taken = lax.ppermute(given, 'tp', swap)  15.7 us
    ppermute x2, starting transfers between devices, from_behind(): lax.ppermute(value, axis, [(source, source + steps) for source in range(f...  6.97 us
  transfers between devices with their start and end apart: 6, of which 2 were waited for; matrix products, arithmetic and copies ran while one was open for 5% of the time, Pallas kernels for 0%

profile of v3, /device:TPU:0, one launch (start us, length us, event | category | flops | bytes accessed | tf_op | source)
XLA Modules:
  0.0 197.1 jit_solution(3732492793095198675)
XLA Ops:
  0.0 0.0 copy-start.2
  0.0 1.2 multiply_convert_fusion.1
  1.2 2.4 %collective-permute-start.2 = (bf16[2,512]{1,0:T(2,128)(2,1)S(1)}, bf16[2,512]{1,0:T(2,128)(2,1)S(1)}, u32[]{:S(2)}, u32[]{:S(2)}) collective-permute-start(bf16[2,512]{1,0:T(2,128)(2,1)S(1)} %slice.41), channel_id=1, source_target_pairs={{0,2},{2,4},{4,6},{6,8},{8,10},{10,12},{12,14},{1,3},{3,5},{5,7},{... | collective-permute-start | bytes 6152 | tf_op jit(solution)/shard_map/ppermute | solution.py:19
  3.6 0.7 convert.3
  4.3 0.1 slice.31
  4.4 4.6 %collective-permute-start.1 = (bf16[2]{0:T(256)(128)(2,1)S(1)}, bf16[2]{0:T(256)(128)(2,1)S(1)}, u32[]{:S(2)}, u32[]{:S(2)}) collective-permute-start(bf16[2]{0:T(256)(128)(2,1)S(1)} %slice.31), channel_id=1, source_target_pairs={{0,2},{2,4},{4,6},{6,8},{8,10},{10,12},{12,14},{1,3},{3,5},{5,7},{... | collective-permute-start | bytes 20 | tf_op jit(solution)/shard_map/ppermute | solution.py:19
  9.0 1.8 constant_dynamic-slice_fusion.2
  10.8 1.5 collective-permute-start
  12.3 0.5 collective-permute-start.5
  12.8 0.8 fusion.11
  13.6 0.8 constant_dynamic-slice_fusion.1
  14.4 0.8 constant_dynamic-slice_fusion
  15.2 0.1 convolution_select_fusion
  15.4 0.0 collective-permute-done.1
  15.4 0.0 copy-done.2
  15.4 0.1 pad_add_fusion
  15.5 0.1 slice_compare_fusion.1
  15.6 0.0 collective-permute-done.2
  15.6 0.1 maximum_convert_fusion
  15.7 0.0 copy-start.4
  15.7 0.0 copy-start
  15.7 1.7 multiply_reduce_fusion
  17.4 1.5 collective-permute-start.3
  19.0 0.6 pad.4.own_meta
  19.6 2.6 %collective-permute-done.3 = f32[384]{0:T(512)S(1)} collective-permute-done((f32[384]{0:T(512)S(1)}, f32[384]{0:T(512)S(1)}, u32[]{:S(2)}, u32[]{:S(2)}) %collective-permute-start.3) | collective-permute-done | bytes 1568 | tf_op jit(solution)/shard_map/ppermute | solution.py:557
  22.2 0.0 copy-done.4
  22.2 0.1 multiply_convert_fusion
  22.3 0.0 copy-done
  22.3 0.6 convolution_convert_fusion
  22.9 0.0 copy-start.3
  22.9 0.0 copy-start.1
  22.9 1.6 collective-permute-start.4
  24.5 0.6 convolution_convert_fusion.1
  25.1 0.0 collective-permute-done.5
  25.1 0.0 copy-done.3
  25.1 0.6 pad_maximum_fusion
  25.7 0.0 collective-permute-done
  25.7 0.0 copy-done.1
  25.7 0.2 broadcast_select_fusion.1
  25.9 15.7 %collective-permute-done.4 = bf16[192,2048]{1,0:T(8,128)(2,1)S(1)} collective-permute-done((bf16[192,2048]{1,0:T(8,128)(2,1)S(1)}, bf16[192,2048]{1,0:T(8,128)(2,1)S(1)}, u32[]{:S(2)}, u32[]{:S(2)}) %collective-permute-start.4) | collective-permute-done | bytes 786464 | tf_op jit(solution)/shard_map/ppermute | solution.py:566
  41.6 1.3 add_convert_fusion.own_ref
  42.9 152.2 %shard_map.163 = bf16[2,192,1024]{2,1,0:T(8,128)(2,1)} custom-call(bf16[192,2048]{1,0:T(8,128)(2,1)} %add_convert_fusion.own_ref, f32[4,8,256]{2,1,0:T(8,128)} %pad.4.own_meta, f32[1,2048]{1,0:T(1,128)} %bitcast.19, bf16[2,2048,256]{2,1,0:T(8,128)(2,1)} %wg_hbm.1, bf16[2,2048,256]{2,1,0:T(8,128)(2,1)} %wu_hbm.1, bf16[2,512,1024]{2,1,0:T(8,128)(2,1)} %wd_hbm.1, ...), custom_call_target="tpu_custom_call" | custom-call | tf_op jit(solution)/shard_map/pallas_call | solution.py:593
  195.1 2.1 %copy.24 = bf16[384,1024]{1,0:T(8,128)(2,1)} copy(bf16[384,1024]{1,0:T(8,128)(2,1)} %bitcast.16) | data formatting | bytes 1572864
  (10 shorter events, 0.1 us)
Async XLA Ops:
  0.0 15.4 %copy-start.2 = (s32[384]{0:T(512)S(1)}, s32[384]{0:T(512)}, u32[]{:S(2)}) copy-start(s32[384]{0:T(512)} %param.20) | copy-start | bytes 4612
  1.2 14.3 %collective-permute-start.2 = (bf16[2,512]{1,0:T(2,128)(2,1)S(1)}, bf16[2,512]{1,0:T(2,128)(2,1)S(1)}, u32[]{:S(2)}, u32[]{:S(2)}) collective-permute-start(bf16[2,512]{1,0:T(2,128)(2,1)S(1)} %slice.41), channel_id=1, source_target_pairs={{0,2},{2,4},{4,6},{6,8},{8,10},{10,12},{12,14},{1,3},{3,5},{5,7},{... | collective-permute-start | bytes 6152 | tf_op jit(solution)/shard_map/ppermute | solution.py:19
  4.4 11.0 %collective-permute-start.1 = (bf16[2]{0:T(256)(128)(2,1)S(1)}, bf16[2]{0:T(256)(128)(2,1)S(1)}, u32[]{:S(2)}, u32[]{:S(2)}) collective-permute-start(bf16[2]{0:T(256)(128)(2,1)S(1)} %slice.31), channel_id=1, source_target_pairs={{0,2},{2,4},{4,6},{6,8},{8,10},{10,12},{12,14},{1,3},{3,5},{5,7},{... | collective-permute-start | bytes 20 | tf_op jit(solution)/shard_map/ppermute | solution.py:19
  10.8 14.9 %collective-permute-start = (bf16[192,1024]{1,0:T(8,128)(2,1)}, bf16[192,1024]{1,0:T(8,128)(2,1)S(1)}, u32[]{:S(2)}, u32[]{:S(2)}) collective-permute-start(bf16[192,1024]{1,0:T(8,128)(2,1)} %constant_dynamic-slice_fusion.2), channel_id=1, source_target_pairs={{0,1},{1,0},{2,3},{3,2},{4,5},{5,4},{6,7},{7,6},{8,9},{9,8},{10,11... | collective-permute-start | bytes 1179656 | tf_op jit(solution)/shard_map/ppermute | solution.py:544
  12.3 12.8 %collective-permute-start.5 = (f32[1024]{0:T(1024)}, f32[1024]{0:T(1024)S(1)}, u32[]{:S(2)}, u32[]{:S(2)}) collective-permute-start(f32[1024]{0:T(1024)} %param.25), channel_id=1, source_target_pairs={{0,1},{1,0},{2,3},{3,2},{4,5},{5,4},{6,7},{7,6},{8,9},{9,8},{10,11... | collective-permute-start | bytes 12296 | tf_op jit(solution)/shard_map/ppermute | solution.py:558
  15.7 6.5 %copy-start.4 = (f32[512]{0:T(512)S(1)}, f32[512]{0:T(512)}, u32[]{:S(2)}) copy-start(f32[512]{0:T(512)} %param.23) | copy-start | bytes 6148
  15.7 6.6 %copy-start = (bf16[512,2048]{1,0:T(8,128)(2,1)S(1)}, bf16[512,2048]{1,0:T(8,128)(2,1)}, u32[]{:S(2)}) copy-start(bf16[512,2048]{1,0:T(8,128)(2,1)} %param.24) | copy-start | bytes 6291460
  17.4 4.8 %collective-permute-start.3 = (f32[384]{0:T(512)S(1)}, f32[384]{0:T(512)S(1)}, u32[]{:S(2)}, u32[]{:S(2)}) collective-permute-start(f32[384]{0:T(512)S(1)} %get-tuple-element.5), channel_id=1, source_target_pairs={{0,1},{1,0},{2,3},{3,2},{4,5},{5,4},{6,7},{7,6},{8,9},{9,8},{10,11... | collective-permute-start | bytes 4616 | tf_op jit(solution)/shard_map/ppermute | solution.py:557
  22.9 2.2 %copy-start.3 = (f32[1024]{0:T(1024)S(1)}, f32[1024]{0:T(1024)}, u32[]{:S(2)}) copy-start(f32[1024]{0:T(1024)} %param.25) | copy-start | bytes 12292
  22.9 2.8 %copy-start.1 = (bf16[384,1024]{1,0:T(8,128)(2,1)S(1)}, bf16[384,1024]{1,0:T(8,128)(2,1)}, u32[]{:S(2)}) copy-start(bf16[384,1024]{1,0:T(8,128)(2,1)} %param.21) | copy-start | bytes 2359300
  22.9 18.7 %collective-permute-start.4 = (bf16[192,2048]{1,0:T(8,128)(2,1)S(1)}, bf16[192,2048]{1,0:T(8,128)(2,1)S(1)}, u32[]{:S(2)}, u32[]{:S(2)}) collective-permute-start(bf16[192,2048]{1,0:T(8,128)(2,1)S(1)} %convolution_convert_fusion), channel_id=1, source_target_pairs={{0,1},{1,0},{2,3},{3,2},{4,5},{5,4},{6,7},{7,6},{8,9},{9,8},{10,11... | collective-permute-start | bytes 2359304 | tf_op jit(solution)/shard_map/ppermute | solution.py:566

commit v4 on v3

--- a/solution.py
+++ b/solution.py
@@ -389,6 +389,18 @@
             start(b, 2)
             start(b, 3)
 
+        @pl.when(valid(i - 4))
+        def _():
+            zq = zone(i - 4)
+            results(zq)
+
+            @pl.when(is_end(zq))
+            def _():
+                sib_copy(zq).wait_recv()
+                for q in range(2 * per):
+                    acc[zq, q] = (acc[zq, q].astype(F32) + sib[zq, q].astype(F32)).astype(BF16)
+                    pass_on(zq, q)
+
         @pl.when(valid(i - 2))
         def _():
             zq = zone(i - 2)
@@ -410,17 +422,6 @@
         def _():
             sh_copy().start()
 
-        @pl.when(valid(i - 4))
-        def _():
-            zq = zone(i - 4)
-            results(zq)
-
-            @pl.when(is_end(zq))
-            def _():
-                sib_copy(zq).wait_recv()
-                for q in range(2 * per):
-                    acc[zq, q] = (acc[zq, q].astype(F32) + sib[zq, q].astype(F32)).astype(BF16)
-                    pass_on(zq, q)
 
     above = n_z - 1 - z
     up_first = (above >= z).astype(jnp.int32)
@@ -584,7 +585,7 @@
     pad = -rows % 128
     info = jnp.pad(info, ((0, 0), (0, 0), (0, pad)), constant_values=-1.0)
 
-    per = 4 if rows % 64 == 0 else 1
+    per = 2
     piece = rows // per
     blocks = n_sp * n_tp
     half = expert_gate.shape[2]

time: 198 us -> 192 us (0.970)
  Pallas kernels: 152 us -> 146 us
    pallas_call x1, Pallas kernels: 152 us -> 146 us  [fast(): pl.pallas_call(functools.partial(moe_kernel, n_z, most), out_shape=jax.Sh...]
where the time goes in v4:
time: 192 us; the launch traced here: 191 us
  Pallas kernels  146 us (76%)
  waiting for transfers between devices  18.3 us (10%)
  starting transfers between devices  12.1 us (6%)
  local copies, waits for them, and re-layouts  6.96 us (4%)
  other arithmetic  6.1 us (3%)
    pallas_call x1, Pallas kernels, fast(): pl.pallas_call(functools.partial(moe_kernel, n_z, most), out_shape=jax.Sh...  146 us
    ppermute x1, waiting for transfers between devices, fast(): taken = lax.ppermute(given, 'tp', swap)  15.7 us
    ppermute x2, starting transfers between devices, from_behind(): lax.ppermute(value, axis, [(source, source + steps) for source in range(f...  6.97 us
  transfers between devices with their start and end apart: 6, of which 2 were waited for; matrix products, arithmetic and copies ran while one was open for 5% of the time, Pallas kernels for 0%

profile of v4, /device:TPU:0, one launch (start us, length us, event | category | flops | bytes accessed | tf_op | source)
XLA Modules:
  0.0 190.8 jit_solution(10625317994958233755)
XLA Ops:
  0.0 0.0 copy-start.2
  0.0 1.2 multiply_convert_fusion.1
  1.2 2.4 %collective-permute-start.2 = (bf16[2,512]{1,0:T(2,128)(2,1)S(1)}, bf16[2,512]{1,0:T(2,128)(2,1)S(1)}, u32[]{:S(2)}, u32[]{:S(2)}) collective-permute-start(bf16[2,512]{1,0:T(2,128)(2,1)S(1)} %slice.41), channel_id=1, source_target_pairs={{0,2},{2,4},{4,6},{6,8},{8,10},{10,12},{12,14},{1,3},{3,5},{5,7},{... | collective-permute-start | bytes 6152 | tf_op jit(solution)/shard_map/ppermute | solution.py:19
  3.6 0.7 convert.3
  4.3 0.1 slice.31
  4.4 4.6 %collective-permute-start.1 = (bf16[2]{0:T(256)(128)(2,1)S(1)}, bf16[2]{0:T(256)(128)(2,1)S(1)}, u32[]{:S(2)}, u32[]{:S(2)}) collective-permute-start(bf16[2]{0:T(256)(128)(2,1)S(1)} %slice.31), channel_id=1, source_target_pairs={{0,2},{2,4},{4,6},{6,8},{8,10},{10,12},{12,14},{1,3},{3,5},{5,7},{... | collective-permute-start | bytes 20 | tf_op jit(solution)/shard_map/ppermute | solution.py:19
  9.0 1.8 constant_dynamic-slice_fusion.2
  10.8 1.5 collective-permute-start
  12.3 0.5 collective-permute-start.5
  12.8 0.8 fusion.11
  13.6 0.8 constant_dynamic-slice_fusion.1
  14.4 0.8 constant_dynamic-slice_fusion
  15.2 0.1 convolution_select_fusion
  15.4 0.0 collective-permute-done.1
  15.4 0.0 copy-done.2
  15.4 0.1 pad_add_fusion
  15.5 0.1 slice_compare_fusion.1
  15.6 0.0 collective-permute-done.2
  15.6 0.1 maximum_convert_fusion
  15.7 0.0 copy-start.4
  15.7 0.0 copy-start
  15.7 1.7 multiply_reduce_fusion
  17.4 1.5 collective-permute-start.3
  19.0 0.6 pad.4.own_meta
  19.6 2.6 %collective-permute-done.3 = f32[384]{0:T(512)S(1)} collective-permute-done((f32[384]{0:T(512)S(1)}, f32[384]{0:T(512)S(1)}, u32[]{:S(2)}, u32[]{:S(2)}) %collective-permute-start.3) | collective-permute-done | bytes 1568 | tf_op jit(solution)/shard_map/ppermute | solution.py:558
  22.2 0.0 copy-done.4
  22.2 0.1 multiply_convert_fusion
  22.3 0.0 copy-done
  22.3 0.6 convolution_convert_fusion
  22.9 0.0 copy-start.3
  22.9 0.0 copy-start.1
  22.9 1.6 collective-permute-start.4
  24.5 0.6 convolution_convert_fusion.1
  25.1 0.0 collective-permute-done.5
  25.1 0.0 copy-done.3
  25.1 0.6 pad_maximum_fusion
  25.7 0.0 collective-permute-done
  25.7 0.0 copy-done.1
  25.7 0.2 broadcast_select_fusion.1
  25.9 15.7 %collective-permute-done.4 = bf16[192,2048]{1,0:T(8,128)(2,1)S(1)} collective-permute-done((bf16[192,2048]{1,0:T(8,128)(2,1)S(1)}, bf16[192,2048]{1,0:T(8,128)(2,1)S(1)}, u32[]{:S(2)}, u32[]{:S(2)}) %collective-permute-start.4) | collective-permute-done | bytes 786464 | tf_op jit(solution)/shard_map/ppermute | solution.py:567
  41.6 1.3 add_convert_fusion.own_ref
  42.9 145.9 %shard_map.163 = bf16[2,192,1024]{2,1,0:T(8,128)(2,1)} custom-call(bf16[192,2048]{1,0:T(8,128)(2,1)} %add_convert_fusion.own_ref, f32[4,8,256]{2,1,0:T(8,128)} %pad.4.own_meta, f32[1,2048]{1,0:T(1,128)} %bitcast.19, bf16[2,2048,256]{2,1,0:T(8,128)(2,1)} %wg_hbm.1, bf16[2,2048,256]{2,1,0:T(8,128)(2,1)} %wu_hbm.1, bf16[2,512,1024]{2,1,0:T(8,128)(2,1)} %wd_hbm.1, ...), custom_call_target="tpu_custom_call" | custom-call | tf_op jit(solution)/shard_map/pallas_call | solution.py:594
  188.7 2.1 %copy.24 = bf16[384,1024]{1,0:T(8,128)(2,1)} copy(bf16[384,1024]{1,0:T(8,128)(2,1)} %bitcast.16) | data formatting | bytes 1572864
  (10 shorter events, 0.1 us)
Async XLA Ops:
  0.0 15.4 %copy-start.2 = (s32[384]{0:T(512)S(1)}, s32[384]{0:T(512)}, u32[]{:S(2)}) copy-start(s32[384]{0:T(512)} %param.20) | copy-start | bytes 4612
  1.2 14.3 %collective-permute-start.2 = (bf16[2,512]{1,0:T(2,128)(2,1)S(1)}, bf16[2,512]{1,0:T(2,128)(2,1)S(1)}, u32[]{:S(2)}, u32[]{:S(2)}) collective-permute-start(bf16[2,512]{1,0:T(2,128)(2,1)S(1)} %slice.41), channel_id=1, source_target_pairs={{0,2},{2,4},{4,6},{6,8},{8,10},{10,12},{12,14},{1,3},{3,5},{5,7},{... | collective-permute-start | bytes 6152 | tf_op jit(solution)/shard_map/ppermute | solution.py:19
  4.4 11.0 %collective-permute-start.1 = (bf16[2]{0:T(256)(128)(2,1)S(1)}, bf16[2]{0:T(256)(128)(2,1)S(1)}, u32[]{:S(2)}, u32[]{:S(2)}) collective-permute-start(bf16[2]{0:T(256)(128)(2,1)S(1)} %slice.31), channel_id=1, source_target_pairs={{0,2},{2,4},{4,6},{6,8},{8,10},{10,12},{12,14},{1,3},{3,5},{5,7},{... | collective-permute-start | bytes 20 | tf_op jit(solution)/shard_map/ppermute | solution.py:19
  10.8 14.9 %collective-permute-start = (bf16[192,1024]{1,0:T(8,128)(2,1)}, bf16[192,1024]{1,0:T(8,128)(2,1)S(1)}, u32[]{:S(2)}, u32[]{:S(2)}) collective-permute-start(bf16[192,1024]{1,0:T(8,128)(2,1)} %constant_dynamic-slice_fusion.2), channel_id=1, source_target_pairs={{0,1},{1,0},{2,3},{3,2},{4,5},{5,4},{6,7},{7,6},{8,9},{9,8},{10,11... | collective-permute-start | bytes 1179656 | tf_op jit(solution)/shard_map/ppermute | solution.py:545
  12.3 12.8 %collective-permute-start.5 = (f32[1024]{0:T(1024)}, f32[1024]{0:T(1024)S(1)}, u32[]{:S(2)}, u32[]{:S(2)}) collective-permute-start(f32[1024]{0:T(1024)} %param.25), channel_id=1, source_target_pairs={{0,1},{1,0},{2,3},{3,2},{4,5},{5,4},{6,7},{7,6},{8,9},{9,8},{10,11... | collective-permute-start | bytes 12296 | tf_op jit(solution)/shard_map/ppermute | solution.py:559
  15.7 6.5 %copy-start.4 = (f32[512]{0:T(512)S(1)}, f32[512]{0:T(512)}, u32[]{:S(2)}) copy-start(f32[512]{0:T(512)} %param.23) | copy-start | bytes 6148
  15.7 6.6 %copy-start = (bf16[512,2048]{1,0:T(8,128)(2,1)S(1)}, bf16[512,2048]{1,0:T(8,128)(2,1)}, u32[]{:S(2)}) copy-start(bf16[512,2048]{1,0:T(8,128)(2,1)} %param.24) | copy-start | bytes 6291460
  17.4 4.8 %collective-permute-start.3 = (f32[384]{0:T(512)S(1)}, f32[384]{0:T(512)S(1)}, u32[]{:S(2)}, u32[]{:S(2)}) collective-permute-start(f32[384]{0:T(512)S(1)} %get-tuple-element.5), channel_id=1, source_target_pairs={{0,1},{1,0},{2,3},{3,2},{4,5},{5,4},{6,7},{7,6},{8,9},{9,8},{10,11... | collective-permute-start | bytes 4616 | tf_op jit(solution)/shard_map/ppermute | solution.py:558
  22.9 2.2 %copy-start.3 = (f32[1024]{0:T(1024)S(1)}, f32[1024]{0:T(1024)}, u32[]{:S(2)}) copy-start(f32[1024]{0:T(1024)} %param.25) | copy-start | bytes 12292
  22.9 2.8 %copy-start.1 = (bf16[384,1024]{1,0:T(8,128)(2,1)S(1)}, bf16[384,1024]{1,0:T(8,128)(2,1)}, u32[]{:S(2)}) copy-start(bf16[384,1024]{1,0:T(8,128)(2,1)} %param.21) | copy-start | bytes 2359300
  22.9 18.7 %collective-permute-start.4 = (bf16[192,2048]{1,0:T(8,128)(2,1)S(1)}, bf16[192,2048]{1,0:T(8,128)(2,1)S(1)}, u32[]{:S(2)}, u32[]{:S(2)}) collective-permute-start(bf16[192,2048]{1,0:T(8,128)(2,1)S(1)} %convolution_convert_fusion), channel_id=1, source_target_pairs={{0,1},{1,0},{2,3},{3,2},{4,5},{5,4},{6,7},{7,6},{8,9},{9,8},{10,11... | collective-permute-start | bytes 2359304 | tf_op jit(solution)/shard_map/ppermute | solution.py:567
